TPU v7x, 256 devices: a whole 4x4x8 slice. The times are simulated.
256 devices in a mesh: sp: 32 (over z, y), tp: 8 (over x, core).
Axes of the slice: x: 4, y: 4, z: 8, core: 2. Of those that a mesh axis runs over, the one named last changes fastest.
Arguments:
- hidden: bfloat16 [4096, 2048], P('sp'), may hold values from -6 to 6
- value_weight: bfloat16 [2048, 4096], P(None, 'tp'), may hold values from -0.125 to 0.125
- key_vecs: bfloat16 [4096, 8, 128], P('sp', 'tp'), may hold values from -0.29882812 to 0.29882812
- queries: bfloat16 [4096, 8, 128], P('sp', 'tp'), may hold values from -0.29882812 to 0.29882812
- decay_pre: float32 [4096, 64], P('sp', 'tp'), may hold values from -4 to 4
- decay_rate: float32 [64], P('tp'), may hold values from 1.4648437e-05 to 0.0009033203
- cotangent: bfloat16 [4096, 64, 64], P('sp', 'tp'), may hold values from -1.1953125 to 1.1953125
Outputs:
- grad_keys: bfloat16 [4096, 8, 128], P('sp', 'tp')
- grad_queries: bfloat16 [4096, 8, 128], P('sp', 'tp')
- grad_decay: float32 [4096, 64], P('sp', 'tp')
- grad_hidden: bfloat16 [4096, 2048], P(('sp', 'tp'))
- grad_weight: float32 [2048, 4096], P('sp', 'tp')
All inputs are finite; a program needn't handle non-finite values.
Results may differ from a plain program's by a relative error of at most 0.003.
Values sent between devices are 32-bit elements.
A program may use at most 64 MiB of HBM per device.

v0:
```python
import jax
import jax.numpy as jnp
from jax import lax
from jax.sharding import Mesh
from jax.sharding import PartitionSpec as P

SP = ("sp_0", "sp_1")
SP_TP = ("sp_0", "sp_1", "tp")


highest = lax.Precision.HIGHEST


def filled_with(array, identity):
    return jax.tree.map(
        lambda a, e: jnp.broadcast_to(jnp.asarray(e, a.dtype), a.shape), array, identity
    )


def carried_in(array, axes, combine, identity, reverse):
    before = start = filled_with(array, identity)
    running = array
    for axis in reversed(axes):
        peers, here = lax.axis_size(axis), lax.axis_index(axis)
        pieces = jax.tree.map(lambda part: lax.all_gather(part, axis), running)
        inside, running = start, start
        for k in reversed(range(peers)) if reverse else range(peers):
            passed = k > here if reverse else k < here
            running = combine(running, jax.tree.map(lambda part: part[k], pieces))
            inside = jax.tree.map(lambda new, old: jnp.where(passed, new, old), running, inside)
        before = combine(inside, before)
    return before


def summed_rows(portion, span, axis):
    count = span * lax.axis_size(axis)
    return lax.psum_scatter(portion(jnp.int32(0), count), axis, scatter_dimension=0, tiled=True)


def summed_rows_2(product, span, axes):
    running = product(jnp.int32(0), span * lax.axis_size(axes))
    for axis in axes:
        running = lax.psum_scatter(running, axis, scatter_dimension=0, tiled=True)
    return running


def local_mixer(values_f, keys_f, queries_f, decay_pre, decay_rate, state_in):
    heads_here = values_f.shape[1]
    per_group = heads_here // keys_f.shape[1]
    key_heads = jnp.repeat(keys_f, per_group, axis=1)
    query_heads = jnp.repeat(queries_f, per_group, axis=1)
    log_decay = -decay_rate[None, :] * jax.nn.softplus(decay_pre)
    cumulative = jnp.cumsum(log_decay, axis=0)
    length = values_f.shape[0]
    causal = jnp.tril(jnp.ones((length, length), dtype=bool))[None]
    across = cumulative.T[:, :, None] - cumulative.T[:, None, :]
    damping = jnp.where(causal, jnp.exp(jnp.where(causal, across, 0.0)), 0.0)
    scores = jnp.einsum("thn,shn->hts", query_heads, key_heads, precision=highest)
    outputs = jnp.einsum("hts,shp->thp", scores * damping, values_f, precision=highest)
    carried = jnp.einsum("thn,hpn->thp", query_heads, state_in, precision=highest)
    outputs = outputs + jnp.exp(cumulative)[:, :, None] * carried
    to_end = jnp.exp(cumulative[-1][None, :] - cumulative)
    state_out = jnp.exp(cumulative[-1])[:, None, None] * state_in + jnp.einsum(
        "sh,shp,shn->hpn", to_end, values_f, key_heads, precision=highest
    )
    return (outputs, state_out)


def chain_combine(earlier, later):
    return (earlier[0] * later[0], later[0][:, None, None] * earlier[1] + later[1])


def local(hidden, value_weight, key_vecs, queries, decay_pre, decay_rate, cotangent):
    length = hidden.shape[0]
    heads_here = decay_rate.shape[0]
    head_width = cotangent.shape[2]
    values = jnp.dot(hidden, value_weight, preferred_element_type=jnp.float32).astype(jnp.bfloat16)
    values_f = values.reshape(length, heads_here, head_width).astype(jnp.float32)
    keys_f = key_vecs.astype(jnp.float32)
    queries_f = queries.astype(jnp.float32)
    grads_out = cotangent.astype(jnp.float32)
    per_group = heads_here // keys_f.shape[1]
    key_heads = jnp.repeat(keys_f, per_group, axis=1)
    query_heads = jnp.repeat(queries_f, per_group, axis=1)
    cumulative = jnp.cumsum(-decay_rate[None, :] * jax.nn.softplus(decay_pre), axis=0)
    decay_total = cumulative[-1]
    to_end = jnp.exp(decay_total[None, :] - cumulative)
    local_state = jnp.einsum("sh,shp,shn->hpn", to_end, values_f, key_heads, precision=highest)
    local_pull = jnp.einsum(
        "th,thp,thn->hpn", jnp.exp(cumulative), grads_out, query_heads, precision=highest
    )
    factor = jnp.exp(decay_total)
    identity_pair = (jnp.ones_like(factor), jnp.zeros_like(local_state))
    state_in = carried_in((factor, local_state), SP, chain_combine, identity_pair, False)[1]
    state_grad = carried_in((factor, local_pull), SP, chain_combine, identity_pair, True)[1]

    def local_part(values_in, keys_in, queries_in, pre_in):
        return local_mixer(values_in, keys_in, queries_in, pre_in, decay_rate, state_in)

    primal, pullback = jax.vjp(local_part, values_f, keys_f, queries_f, decay_pre)
    grad_values, grad_keys, grad_queries, grad_decay = pullback((grads_out, state_grad))
    grad_flat = grad_values.reshape(length, -1).astype(jnp.bfloat16)

    def input_term(start, count):
        rows_now = lax.dynamic_slice_in_dim(grad_flat, start, count, 0)
        return lax.dot_general(
            rows_now, value_weight, (((1,), (1,)), ((), ())), preferred_element_type=jnp.float32
        )

    grad_hidden = summed_rows(input_term, length // lax.axis_size("tp"), "tp").astype(jnp.bfloat16)

    def weight_term(start, count):
        columns = lax.dynamic_slice_in_dim(hidden, start, count, 1)
        return lax.dot_general(
            columns, grad_flat, (((0,), (0,)), ((), ())), preferred_element_type=jnp.float32
        )

    grad_weight = summed_rows_2(weight_term, hidden.shape[1] // lax.axis_size(SP), SP)
    return (
        grad_keys.astype(jnp.bfloat16),
        grad_queries.astype(jnp.bfloat16),
        grad_decay,
        grad_hidden,
        grad_weight,
    )


def solution(mesh):
    split = Mesh(mesh.devices.reshape(8, 4, mesh.shape["tp"]), ("sp_0", "sp_1", "tp"))
    placed = (
        P(SP, None),
        P(None, "tp"),
        P(SP, "tp", None),
        P(SP, "tp", None),
        P(SP, "tp"),
        P("tp"),
        P(SP, "tp", None),
    )
    return jax.shard_map(
        local,
        mesh=split,
        in_specs=placed,
        out_specs=(P(SP, "tp", None), P(SP, "tp", None), P(SP, "tp"), P(SP_TP, None), P(SP, "tp")),
        check_vma=False,
    )
```

profile of v0, /device:TPU:2, one launch (start us, length us, event | category | flops | bytes accessed | tf_op | source)
XLA Modules:
  0.0 290.5 jit_solution(1704536160360201677)
XLA Ops:
  7.2 1.4 broadcast_compare_fusion
  11.4 1.5 convolution_convert_fusion
  15.7 10.0 %all-gather.2 = f32[4,1,8]{2,1,0:T(1,128)S(1)} all-gather(f32[1,1,8]{2,1,0:T(1,128)S(1)} %bitcast.333), channel_id=1, replica_groups=mesh['sp_0'=8,'sp_1'=4,'tp'=8] {'sp_1'}, dimensions={0}, use_global_device_ids=true | all-gather | bytes 160 | tf_op jit(solution)/shard_map/all_gather | solution.py:25
  26.4 17.6 %all-gather.16.cloned.1.call-done = f32[32,64,128]{2,1,0:T(8,128)} async-done(((f32[8,64,128]{2,1,0:T(8,128)}), f32[32,64,128]{2,1,0:T(8,128)}) %all-gather.16.cloned.1.call-update) | async-done | bytes 1048592 | tf_op jit(solution)/shard_map/all_gather | solution.py:25
  44.0 28.9 %all-gather.14.cloned.1.call-done = f32[32,64,128]{2,1,0:T(8,128)} async-done(((f32[8,64,128]{2,1,0:T(8,128)}), f32[32,64,128]{2,1,0:T(8,128)}) %all-gather.14.cloned.1.call-update) | async-done | bytes 1048592 | tf_op jit(solution)/shard_map/all_gather | solution.py:25
  72.9 2.5 bitcast_add_fusion.4
  77.5 16.7 %all-gather.3 = f32[8,1,8]{2,1,0:T(1,128)S(1)} all-gather(f32[1,1,8]{2,1,0:T(1,128)S(1)} %get-tuple-element.61), channel_id=1, replica_groups=mesh['sp_0'=8,'sp_1'=4,'tp'=8] {'sp_0'}, dimensions={0}, use_global_device_ids=true | all-gather | bytes 288 | tf_op jit(solution)/shard_map/all_gather | solution.py:25
  94.1 14.3 %all-gather.4 = f32[8,1,8]{2,1,0:T(1,128)S(1)} all-gather(f32[1,1,8]{2,1,0:T(1,128)S(1)} %get-tuple-element.62), channel_id=1, replica_groups=mesh['sp_0'=8,'sp_1'=4,'tp'=8] {'sp_0'}, dimensions={0}, use_global_device_ids=true | all-gather | bytes 288 | tf_op jit(solution)/shard_map/all_gather | solution.py:25
  110.8 3.4 %fusion.79 = (f32[8,128]{1,0:T(8,128)}, f32[8,128]{1,0:T(8,128)}, f32[8,128,128]{1,2,0:T(8,128)}) fusion(f32[8,128]{1,0:T(8,128)} %copy.106, f32[8,128,128]{1,2,0:T(8,128)S(1)} %convolution_bitcast_fusion.1, pred[128,128]{0,1:T(8,128)(4,1)S(1)} %iota_compare_fusion, f32[128,128]{1,0:T(8,128)} %copy-done.14, f32[128,128]{1,0:T(8,128)S(1)} %bitcast_convert_fusion.1), kind=kOutput, calls=%fused_computation.117 | convolution fusion | flops 202373120 | bytes 1208320 | tf_op jit(solution)/shard_map/jvp(thn,shn->hts)/dot_general | solution.py:58
  114.2 2.8 all-gather.10.cloned.1.call-done
  117.0 40.5 %all-gather.12.cloned.1.call-done = f32[8,8,64,128]{3,2,1,0:T(8,128)} async-done(((f32[1,8,64,128]{3,2,1,0:T(8,128)}), f32[8,8,64,128]{3,2,1,0:T(8,128)}) %all-gather.12.cloned.1.call-update) | async-done | bytes 2097168 | tf_op jit(solution)/shard_map/all_gather | solution.py:25
  157.6 4.4 %multiply_reduce_fusion = (f32[8]{0:T(128)}, f32[8,64,128]{2,1,0:T(8,128)S(1)}, f32[8,64,128]{2,1,0:T(8,128)S(1)}) fusion(pred[]{:T(512)S(6)} %gt.39, pred[]{:T(512)S(6)} %gt.38, pred[]{:T(512)S(6)} %gt.37, f32[32,64,128]{2,1,0:T(8,128)S(1)} %copy-done.1, f32[8]{0:T(128)} %copy-done.27, f32[8]{0:T(128)} %copy-done.30, f32[8]{0:T(128)} %copy-done.31, ...), kind=kLoop, calls=%fused_computation.81 | loop fusion | flops 4849656 | bytes 6816568 | tf_op jit(solution)/shard_map/transpose(jvp())/reduce_sum | solution.py:63
  162.7 1.7 fusion.18
  165.2 2.6 convolution_bitcast_fusion
  167.9 1.8 fusion.92
  170.0 1.4 copy.115
  171.4 2.8 convolution_bitcast_fusion.3
  175.5 1.7 fusion.6
  177.2 1.4 exponential_multiply_fusion
  178.6 43.1 %reduce-scatter.8.cloned.1.call-done = f32[256,512]{0,1:T(8,128)} async-done(((f32[2048,512]{0,1:T(8,128)}), f32[256,512]{0,1:T(8,128)}) %reduce-scatter.8.cloned.1.call-update) | async-done | bytes 524304 | tf_op jit(solution)/shard_map/reduce_scatter | solution.py:43
  221.7 2.0 copy.130
  226.5 1.4 bitcast_add_fusion.8
  227.9 1.4 copy.113
  229.3 2.6 reduce_window_sum.25
  231.9 1.5 fusion.76
  233.4 1.5 copy.120
  234.9 2.1 fusion.1
  237.7 1.7 fusion.16
  239.4 2.5 fusion.2
  241.9 12.5 %reduce-scatter.6.cloned.1.call-done = f32[16,2048]{1,0:T(8,128)} async-done(((f32[128,2048]{1,0:T(8,128)}), f32[16,2048]{1,0:T(8,128)}) %reduce-scatter.6.cloned.1.call-update) | async-done | bytes 131088 | tf_op jit(solution)/shard_map/reduce_scatter | solution.py:37
  254.4 1.5 convert_element_type.63
  255.9 27.7 %reduce-scatter.10.cloned.1.call-done = f32[64,512]{1,0:T(8,128)} async-done(((f32[256,512]{1,0:T(8,128)}), f32[64,512]{1,0:T(8,128)}) %reduce-scatter.10.cloned.1.call-update) | async-done | bytes 131088
  (110 shorter events, 17.0 us)
Async XLA Ops:
  7.2 4.2 %copy-start = (bf16[2048,512]{1,0:T(8,128)(2,1)S(1)}, bf16[2048,512]{1,0:T(8,128)(2,1)}, u32[]{:S(2)}) copy-start(bf16[2048,512]{1,0:T(8,128)(2,1)} %param.8) | copy-start | bytes 6291460
  7.2 5.8 %copy-start.24 = (bf16[128,1,128]{2,0,1:T(8,128)(2,1)S(1)}, bf16[128,1,128]{2,0,1:T(8,128)(2,1)}, u32[]{:S(2)}) copy-start(bf16[128,1,128]{2,0,1:T(8,128)(2,1)} %param.9) | copy-start | bytes 98308
  7.2 36.8 %all-gather.16.cloned.1.call-start = ((), (), s32[]{:S(2)}) async-start(), calls=%async_computation.8 | async-start | bytes 1310720 | tf_op jit(solution)/shard_map/all_gather | solution.py:25
  9.4 4.9 %copy-start.12 = (f32[128,8]{1,0:T(8,128)}, f32[128,8]{1,0:T(8,128)S(1)}, u32[]{:S(2)}) copy-start(f32[128,8]{1,0:T(8,128)S(1)} %copy.101) | copy-start | bytes 12292
  11.3 4.3 %copy-start.17 = (f32[128,8]{0,1:T(8,128)}, f32[128,8]{0,1:T(8,128)S(1)}, u32[]{:S(2)}) copy-start(f32[128,8]{0,1:T(8,128)S(1)} %get-tuple-element.48) | copy-start | bytes 12292
  11.4 4.3 %copy-start.22 = (f32[128,8]{0,1:T(8,128)}, f32[128,8]{0,1:T(8,128)S(1)}, u32[]{:S(2)}) copy-start(f32[128,8]{0,1:T(8,128)S(1)} %get-tuple-element.47) | copy-start | bytes 12292
  14.3 58.5 %all-gather.14.cloned.1.call-start = ((), (), s32[]{:S(2)}) async-start(), calls=%async_computation.7 | async-start | bytes 1310720 | tf_op jit(solution)/shard_map/all_gather | solution.py:25
  14.4 95.6 %copy-start.10 = (f32[128,128]{1,0:T(8,128)}, f32[128,128]{1,0:T(8,128)S(1)}, u32[]{:S(2)}) copy-start(f32[128,128]{1,0:T(8,128)S(1)} %bitcast_convert_fusion.1) | copy-start | bytes 196612
  15.7 101.3 %all-gather.10.cloned.1.call-start = ((), (), s32[]{:S(2)}) async-start(), calls=%async_computation.3 | async-start | bytes 2359296 | tf_op jit(solution)/shard_map/all_gather | solution.py:25
  25.7 47.1 %copy-start.26 = (f32[4,1,8]{2,1,0:T(1,128)}, f32[4,1,8]{2,1,0:T(1,128)S(1)}, u32[]{:S(2)}) copy-start(f32[4,1,8]{2,1,0:T(1,128)S(1)} %all-gather.2) | copy-start | bytes 388
  25.7 47.1 %copy-start.29 = (f32[8]{0:T(128)}, f32[8]{0:T(128)S(1)}, u32[]{:S(2)}) copy-start(f32[8]{0:T(128)S(1)} %get-tuple-element.63) | copy-start | bytes 100
  25.7 47.1 %copy-start.30 = (f32[8]{0:T(128)}, f32[8]{0:T(128)S(1)}, u32[]{:S(2)}) copy-start(f32[8]{0:T(128)S(1)} %get-tuple-element.64) | copy-start | bytes 100
  25.8 47.1 %copy-start.31 = (f32[8]{0:T(128)}, f32[8]{0:T(128)S(1)}, u32[]{:S(2)}) copy-start(f32[8]{0:T(128)S(1)} %get-tuple-element.65) | copy-start | bytes 100
  25.8 47.1 %copy-start.32 = (f32[8]{0:T(128)}, f32[8]{0:T(128)S(1)}, u32[]{:S(2)}) copy-start(f32[8]{0:T(128)S(1)} %get-tuple-element.66) | copy-start | bytes 100
  26.4 46.5 %copy-start.27 = (f32[8]{0:T(128)}, f32[8]{0:T(128)S(1)}, u32[]{:S(2)}) copy-start(f32[8]{0:T(128)S(1)} %get-tuple-element.58) | copy-start | bytes 100
  26.4 46.5 %copy-start.28 = (f32[8]{0:T(128)}, f32[8]{0:T(128)S(1)}, u32[]{:S(2)}) copy-start(f32[8]{0:T(128)S(1)} %get-tuple-element.59) | copy-start | bytes 100
  75.4 82.1 %copy-start.1 = (f32[32,64,128]{2,1,0:T(8,128)S(1)}, f32[32,64,128]{2,1,0:T(8,128)}, u32[]{:S(2)}) copy-start(f32[32,64,128]{2,1,0:T(8,128)} %all-gather.16.cloned.1.call-done) | copy-start | bytes 3145732
  75.4 82.1 %all-gather.12.cloned.1.call-start = ((), (), s32[]{:S(2)}) async-start(), calls=%async_computation.4 | async-start | bytes 2359296 | tf_op jit(solution)/shard_map/all_gather | solution.py:25
  76.0 145.7 %reduce-scatter.8.cloned.1.call-start = ((), (), s32[]{:S(2)}) async-start(), calls=%async_computation.6 | async-start | bytes 4718592 | tf_op jit(solution)/shard_map/reduce_scatter | solution.py:43
  108.4 49.1 %copy-start.20 = (pred[128,128]{0,1:T(8,128)(4,1)}, pred[128,128]{0,1:T(8,128)(4,1)S(1)}, u32[]{:S(2)}) copy-start(pred[128,128]{0,1:T(8,128)(4,1)S(1)} %iota_compare_fusion) | copy-start | bytes 49156
  157.5 5.1 %copy-start.15 = (f32[128,128]{1,0:T(8,128)S(1)}, f32[128,128]{1,0:T(8,128)}, u32[]{:S(2)}) copy-start(f32[128,128]{1,0:T(8,128)} %copy-done.14) | copy-start | bytes 196612
  157.5 6.8 %copy-start.5 = (bf16[128,8,64]{0,2,1:T(8,128)(2,1)S(1)}, bf16[128,8,64]{0,2,1:T(8,128)(2,1)}, u32[]{:S(2)}) copy-start(bf16[128,8,64]{0,2,1:T(8,128)(2,1)} %param.13) | copy-start | bytes 393220
  157.5 6.8 %copy-start.18 = (f32[128,8]{0,1:T(8,128)S(1)}, f32[128,8]{0,1:T(8,128)}, u32[]{:S(2)}) copy-start(f32[128,8]{0,1:T(8,128)} %copy-done.17) | copy-start | bytes 12292
  157.6 6.8 %copy-start.21 = (pred[128,128]{0,1:T(8,128)(4,1)S(1)}, pred[128,128]{0,1:T(8,128)(4,1)}, u32[]{:S(2)}) copy-start(pred[128,128]{0,1:T(8,128)(4,1)} %copy-done.20) | copy-start | bytes 49156
  157.6 6.8 %copy-start.23 = (f32[8,128]{1,0:T(8,128)S(1)}, f32[8,128]{1,0:T(8,128)}, u32[]{:S(2)}) copy-start(f32[8,128]{1,0:T(8,128)} %copy.106) | copy-start | bytes 12292
  157.6 6.8 %copy-start.34 = (f32[8,128,128]{1,2,0:T(8,128)S(1)}, f32[8,128,128]{1,2,0:T(8,128)}, u32[]{:S(2)}) copy-start(f32[8,128,128]{1,2,0:T(8,128)} %get-tuple-element.69) | copy-start | bytes 1572868
  167.9 7.6 %copy-start.6 = (bf16[128,8,64]{0,2,1:T(8,128)(2,1)S(1)}, bf16[128,8,64]{0,2,1:T(8,128)(2,1)}, u32[]{:S(2)}) copy-start(bf16[128,8,64]{0,2,1:T(8,128)(2,1)} %param.13) | copy-start | bytes 393220
  167.9 86.5 %reduce-scatter.6.cloned.1.call-start = ((), (), s32[]{:S(2)}) async-start(), calls=%async_computation.5 | async-start | bytes 1179648 | tf_op jit(solution)/shard_map/reduce_scatter | solution.py:37
  169.7 62.1 %copy-start.13 = (f32[128,8]{1,0:T(8,128)S(1)}, f32[128,8]{1,0:T(8,128)}, u32[]{:S(2)}) copy-start(f32[128,8]{1,0:T(8,128)} %copy-done.12) | copy-start | bytes 12292
  169.7 65.2 %copy-start.3 = (f32[8,64,128]{2,1,0:T(8,128)S(1)}, f32[8,64,128]{2,1,0:T(8,128)}, u32[]{:S(2)}) copy-start(f32[8,64,128]{2,1,0:T(8,128)} %copy-done.2) | copy-start | bytes 786436
  169.8 113.9 %reduce-scatter.10.cloned.1.call-start = ((), (), s32[]{:S(2)}) async-start(), calls=%async_computation.9 | async-start | bytes 655360
  177.2 62.2 %copy-start.16 = (f32[128,128]{1,0:T(8,128)S(1)}, f32[128,128]{1,0:T(8,128)}, u32[]{:S(2)}) copy-start(f32[128,128]{1,0:T(8,128)} %copy-done.14) | copy-start | bytes 196612
  (10 other events, 22.6 us)
Sparse Core Ops, SparseCore 0:
  14.4 29.5 all-gather.15
  45.8 27.0 all-gather.13
  75.6 41.3 all-gather.9
  118.6 38.8 all-gather.11
  168.0 53.6 reduce-scatter.7
  224.1 30.2 reduce-scatter.5
  257.5 26.1 reduce-scatter.9
where the time goes:
time: 291 us
  waiting for transfers between devices  174 us (60%)
  blocking collectives  41 us (14%)
  matrix products  25.4 us (9%)
  other arithmetic  21.6 us (7%)
  between operations  14.5 us (5%)
  local copies, waits for them, and re-layouts  13.9 us (5%)
    all_gather x4, waiting for transfers between devices, carried_in(): pieces = jax.tree.map(lambda part: lax.all_gather(part, axis), running)  89.8 us
    reduce_scatter x1, waiting for transfers between devices, summed_rows_2(): running = lax.psum_scatter(running, axis, scatter_dimension=0, tiled=True)  43.1 us
    all_gather x3, blocking collectives, carried_in(): pieces = jax.tree.map(lambda part: lax.all_gather(part, axis), running)  41 us
    unnamed x8, waiting for transfers between devices  28.3 us
    reduce_scatter x1, waiting for transfers between devices, summed_rows(): lax.psum_scatter(portion(jnp.int32(0), count), axis, scatter_dimension=0,...  12.5 us
    dot_general x3, matrix products, local_mixer(): jnp.einsum('thn,shn->hts', query_heads, key_heads, precision=highest)  8.74 us
    unnamed x74, local copies, waits for them, and re-layouts  7.25 us
  transfers between devices with their start and end apart: 7, of which 7 were waited for; matrix products, arithmetic and copies ran while one was open for 14% of the time, Pallas kernels for 0%

commit v1 on v0

v1 whole, which is shorter than its diff:
```python
import jax
import jax.numpy as jnp
from jax import lax
from jax.experimental import pallas as pl
from jax.experimental.pallas import tpu as pltpu
from jax.sharding import Mesh
from jax.sharding import PartitionSpec as P

F32, BF16 = jnp.float32, jnp.bfloat16
MESH = pl.DeviceIdType.MESH
SP, TP = ("z", "y"), ("x", "c")
NZ, NY, NX = 8, 4, 4
TOK, STATE, PAIRS, HEADS = 128, 128, 4, 8
ROWS = STATE // NZ


def dot(a, b, dims=((1,), (0,))):
    return lax.dot_general(a, b, (dims, ((), ())), preferred_element_type=F32)


def halves(a):
    high = a.astype(BF16)
    return high, (a - high.astype(F32)).astype(BF16)


def dot_fine_right(a, b, dims=((1,), (0,))):
    high, low = halves(b)
    return dot(a, high, dims) + dot(a, low, dims)


def dot_fine_left(a, b, dims=((1,), (0,))):
    high, low = halves(a)
    return dot(high, b, dims) + dot(low, b, dims)


def dot_fine(a, b, dims=((1,), (0,))):
    a_high, a_low = halves(a)
    b_high, b_low = halves(b)
    return dot(a_high, b_high, dims) + dot(a_high, b_low, dims) + dot(a_low, b_high, dims)


def cols(pair):
    return slice(128 * pair, 128 * pair + 128)


def kernel(
    hid, w, k_in, q_in, pre, rate, cot,
    gk_out, gq_out, gd_out, gh_out, gw_out,
    ys_b, yr_b, ys_f, yr_f, zs_b, zr_b, zs_f, zr_f,
    zbs_b, zbr_b, zbs_f, zbr_f, ybs_b, ybr_b, ybs_f, ybr_f,
    hid_t, hid_r, hid_all, ag_s, ag_r, part, ring_s, ring_r,
    gh_s, gh_r, gx_s, gx_r, gv_in, vals, row_sum,
    y_sem, z_sem, ag_sem, ring_sem, d_sem, x_sem,
):
    z, y = lax.axis_index("z"), lax.axis_index("y")
    x, c = lax.axis_index("x"), lax.axis_index("c")
    lane = lax.broadcasted_iota(jnp.int32, (128, 128), 1)
    first_head = lane[0:1, :] < 64
    sent = []

    def peer_y(o):
        return lax.rem(y + o, NY)

    def peer_z(o):
        return lax.rem(z + o, NZ)

    def peer_x(o):
        return lax.rem(x + o, NX)

    def copy(src, dst, s_sem, r_sem, **where):
        return pltpu.make_async_remote_copy(
            src_ref=src, dst_ref=dst, send_sem=s_sem, recv_sem=r_sem, device_id=where, device_id_type=MESH
        )

    def send(src, dst, s_sem, r_sem, **where):
        made = copy(src, dst, s_sem, r_sem, **where)
        made.start()
        sent.append(made)

    def arrived(dst, r_sem):
        copy(dst, dst, r_sem, r_sem, c=1 - c).wait_recv()

    barrier = pltpu.get_barrier_semaphore()
    for o in range(1, NY):
        pl.semaphore_signal(barrier, inc=1, device_id={"y": peer_y(o)}, device_id_type=MESH)
    for o in range(1, NZ):
        pl.semaphore_signal(barrier, inc=1, device_id={"z": peer_z(o)}, device_id_type=MESH)
    for o in range(1, NX):
        pl.semaphore_signal(barrier, inc=1, device_id={"x": peer_x(o)}, device_id_type=MESH)
    pl.semaphore_signal(barrier, inc=1, device_id={"c": 1 - c}, device_id_type=MESH)

    pre_v = pre[...]
    soft = jnp.maximum(pre_v, 0.0) + jnp.log1p(jnp.exp(-jnp.abs(pre_v)))
    cum = -rate[...] * soft
    lane8 = lane[0:8, :]
    for shift in (1, 2, 4, 8, 16, 32, 64):
        cum = cum + jnp.where(lane8 >= shift, pltpu.roll(cum, shift, 1), 0.0)
    total = jnp.broadcast_to(cum[:, 127:128], (8, 128))
    factor = jnp.exp(total)
    cum_t = cum.T
    from_start_t = jnp.exp(cum).T
    to_end_t = jnp.exp(total - cum).T

    def spread(columns, pair):
        return jnp.where(first_head, columns[:, 2 * pair : 2 * pair + 1], columns[:, 2 * pair + 1 : 2 * pair + 2])

    def factor_row(pair):
        return jnp.where(first_head, factor[2 * pair : 2 * pair + 1, :], factor[2 * pair + 1 : 2 * pair + 2, :])

    q, k = q_in[...], k_in[...]
    q_t = q.astype(F32).T.astype(BF16)
    k_t = k.astype(F32).T.astype(BF16)

    for pair in range(PAIRS):
        scaled = spread(from_start_t, pair) * cot[:, cols(pair)].astype(F32)
        ys_b[pair, 0:128, :] = dot_fine_right(q_t, scaled)
        ys_b[pair, 128:136, :] = jnp.broadcast_to(factor_row(pair), (8, 128))
    yr_b[y] = ys_b[y]
    pl.semaphore_wait(barrier, NY + NZ + NX - 2)

    def send_y(kind, src, dst):
        for o in range(1, NY):
            send(src.at[peer_y(o)], dst.at[y], y_sem.at[0, kind, peer_y(o)], y_sem.at[1, kind, y], y=peer_y(o))

    def wait_y(kind, dst):
        for o in range(1, NY):
            arrived(dst.at[peer_y(o)], y_sem.at[1, kind, peer_y(o)])

    def send_z(kind, src, dst):
        for o in range(1, NZ):
            send(src.at[peer_z(o)], dst.at[z], z_sem.at[0, kind, peer_z(o)], z_sem.at[1, kind, z], z=peer_z(o))

    def wait_z(kind, dst):
        for o in range(1, NZ):
            arrived(dst.at[peer_z(o)], z_sem.at[1, kind, peer_z(o)])

    send_y(0, ys_b, yr_b)

    for half in range(2):
        span = slice(256 * half, 256 * half + 256)
        vals[:, span] = dot(hid[...], w[:, span]).astype(BF16)
    for pair in range(PAIRS):
        scaled = spread(to_end_t, pair) * vals[:, cols(pair)].astype(F32)
        ys_f[pair, 0:128, :] = dot_fine_right(k_t, scaled)
        ys_f[pair, 128:136, :] = jnp.broadcast_to(factor_row(pair), (8, 128))
    yr_f[y] = ys_f[y]
    send_y(1, ys_f, yr_f)

    def scan_plane(got, kept, z_send, reverse):
        state, gain = None, None
        order = range(NY - 1, -1, -1) if reverse else range(NY)
        for block in order:
            value, here = got[block, 0:128, :], got[block, 128:129, :]
            if state is None:
                kept[block] = jnp.zeros((128, 128), F32)
                state, gain = value, here
            else:
                kept[block] = state
                state, gain = here * state + value, gain * here
        for row in range(NZ):
            z_send[row, 0:ROWS, :] = state[row * ROWS : row * ROWS + ROWS, :]
            z_send[row, ROWS : ROWS + 8, :] = jnp.broadcast_to(gain, (8, 128))

    def scan_z(got, back, reverse):
        state = None
        for plane in range(NZ - 1, -1, -1) if reverse else range(NZ):
            value, here = got[plane, 0:ROWS, :], got[plane, ROWS : ROWS + 1, :]
            if state is None:
                back[plane] = jnp.zeros((ROWS, 128), F32)
                state = value
            else:
                back[plane] = state
                state = here * state + value

    def finish_plane(got, kept, plane_in, reverse):
        incoming = plane_in[...].reshape(STATE, 128)
        gain = None
        for block in range(NY - 1, -1, -1) if reverse else range(NY):
            kept[block] = kept[block] + (incoming if gain is None else gain * incoming)
            here = got[block, 128:129, :]
            gain = here if gain is None else gain * here

    wait_y(0, yr_b)
    scan_plane(yr_b, ybs_b, zs_b, True)
    zr_b[z] = zs_b[z]
    send_z(0, zs_b, zr_b)

    for block in range(16):
        turned = hid[:, cols(block)].astype(F32).T
        hid_t[block // 2, 2 * (block % 2) : 2 * (block % 2) + 2] = turned.reshape(2, 64, 128)
    for o in range(1, NY):
        send(hid_t.at[:, peer_y(o)], hid_r.at[y], y_sem.at[0, 2, peer_y(o)], y_sem.at[1, 2, y], y=peer_y(o))
    hid_r[y] = hid_t[:, y]

    wait_y(1, yr_f)
    scan_plane(yr_f, ybs_f, zs_f, False)
    zr_f[z] = zs_f[z]
    send_z(1, zs_f, zr_f)

    wait_z(0, zr_b)
    scan_z(zr_b, zbs_b, True)
    zbr_b[z] = zbs_b[z]
    send_z(2, zbs_b, zbr_b)

    score = dot(k, q, ((1,), (1,)))
    causal = lax.broadcasted_iota(jnp.int32, (128, 128), 0) <= lane
    blend = jnp.zeros((128, 128), F32)
    for pair in range(PAIRS):
        cot_pair, val_pair = cot[:, cols(pair)], vals[:, cols(pair)]
        inner = jnp.zeros((128, 128), F32)
        for side in range(2):
            head = 2 * pair + side
            mine = first_head if side == 0 else jnp.logical_not(first_head)
            across = jnp.where(causal, cum[head : head + 1, :] - cum_t[:, head : head + 1], 0.0)
            damping = jnp.where(causal, jnp.exp(across), 0.0)
            weight = score * damping
            cot_head = jnp.where(mine, cot_pair.astype(F32), 0.0).astype(BF16)
            inner = inner + dot_fine_left(weight, cot_head)
            moved = dot(val_pair, cot_head, ((1,), (1,)))
            blend = blend + moved * damping
            row_sum[head : head + 1, :] = jnp.sum(moved * weight, axis=0, keepdims=True)
        gv_in[pair] = inner

    wait_z(2, zbr_b)
    finish_plane(yr_b, ybs_b, zbr_b, True)
    ybr_b[y] = ybs_b[y]
    send_y(3, ybs_b, ybr_b)

    wait_z(1, zr_f)
    scan_z(zr_f, zbs_f, False)
    zbr_f[z] = zbs_f[z]
    send_z(3, zbs_f, zbr_f)

    blend_t = blend.T
    gk = dot_fine_left(blend, q)
    gq = dot_fine_left(blend_t, k)

    wait_y(3, ybr_b)
    for pair in range(PAIRS):
        pull = ybr_b[pair]
        from_state = spread(to_end_t, pair) * dot_fine_right(k, pull)
        gv_out_pair = gv_in[pair] + from_state
        ag_s[pair] = gv_out_pair.astype(BF16).astype(F32)
        for o in range(1, NY):
            send(ag_s.at[pair], ag_r.at[pair, y], ag_sem.at[0, pair, peer_y(o)], ag_sem.at[1, pair, y], y=peer_y(o))
        ag_r[pair, y] = ag_s[pair]
        gv_in[pair] = gv_out_pair
    grad_v = jnp.concatenate([ag_s[pair].astype(BF16) for pair in range(PAIRS)], axis=1)

    for part_now in range(4):
        span = slice(512 * part_now, 512 * part_now + 512)
        gh_s[:, :, :, span] = dot(grad_v, w[span, :], ((1,), (1,))).reshape(NX, 2, 16, 512)
    send(gh_s.at[:, 1 - c], gh_r, d_sem.at[0], d_sem.at[1], c=1 - c)

    wait_z(3, zbr_f)
    finish_plane(yr_f, ybs_f, zbr_f, False)
    ybr_f[y] = ybs_f[y]
    send_y(4, ybs_f, ybr_f)

    wait_y(2, hid_r)
    for block in range(NY):
        hid_all[:, cols(block)] = hid_r[block].reshape(512, 128).astype(BF16)

    def steps(pair, way):
        return 4 if (pair + way) % 2 == 0 else 3

    def ring_target(pair, way, step):
        n = steps(pair, way)
        return peer_z(n - step) if way == 0 else peer_z(NZ - n + step)

    def ring_send(src, pair, way, step):
        send(
            src, ring_r.at[way, pair, step], ring_sem.at[0, way, pair, step], ring_sem.at[1, way, pair, step],
            z=peer_z(1) if way == 0 else peer_z(NZ - 1),
        )

    def ring_step(pair, way, step):
        arrived(ring_r.at[way, pair, step - 1], ring_sem.at[1, way, pair, step - 1])
        if step < steps(pair, way):
            ring_s[way, pair, step] = ring_r[way, pair, step - 1] + part[pair, ring_target(pair, way, step)]
            ring_send(ring_s.at[way, pair, step], pair, way, step)

    for pair in range(PAIRS):
        for o in range(1, NY):
            arrived(ag_r.at[pair, peer_y(o)], ag_sem.at[1, pair, peer_y(o)])
        gathered = ag_r[pair].reshape(512, 128).astype(BF16)
        part[pair] = dot(hid_all[...], gathered).reshape(NZ, 64, 128)
        for way in range(2):
            ring_send(part.at[pair, ring_target(pair, way, 0)], pair, way, 0)
        if pair == 0:
            arrived(gh_r, d_sem.at[1])
            gx_s[...] = gh_s[:, c] + gh_r[...]
            for o in range(1, NX):
                send(gx_s.at[peer_x(o)], gx_r.at[x], x_sem.at[0, peer_x(o)], x_sem.at[1, x], x=peer_x(o))
            gx_r[x] = gx_s[x]

    for step in range(1, 4):
        for pair in range(PAIRS):
            for way in range(2):
                if step <= steps(pair, way):
                    ring_step(pair, way, step)
        if step == 1:
            wait_y(4, ybr_f)
            gap = jnp.zeros((8, 128), F32)
            shared = jnp.zeros((8, 128), F32)
            head_row = lax.broadcasted_iota(jnp.int32, (8, 128), 0)
            for pair in range(PAIRS):
                carry, pull = ybr_f[pair], ybr_b[pair]
                cot_f = cot[:, cols(pair)].astype(F32)
                val_f = vals[:, cols(pair)].astype(F32)
                cot_scaled = spread(from_start_t, pair) * cot_f
                val_scaled = spread(to_end_t, pair) * val_f
                gq = gq + dot_fine(cot_scaled, carry, ((1,), (1,)))
                gk = gk + dot_fine(val_scaled, pull, ((1,), (1,)))
                out_carried = dot_fine_right(q, carry)
                from_state = dot_fine_right(k, pull)
                owner = head_row == 2 * pair + (lane8 >= 64).astype(jnp.int32)
                chooser = jnp.where(owner, 1.0, 0.0)
                change = cot_scaled * out_carried - val_f * gv_in[pair]
                gap = gap + lax.dot_general(
                    chooser, change, (((1,), (1,)), ((), ())),
                    precision=lax.Precision.HIGHEST, preferred_element_type=F32,
                )
                whole = jnp.sum(val_scaled * from_state, axis=0, keepdims=True)
                whole = whole + factor_row(pair) * jnp.sum(carry * pull, axis=0, keepdims=True)
                shared = shared + jnp.sum(chooser * whole, axis=1, keepdims=True)
            gap = gap + row_sum[...]
            for shift in (1, 2, 4, 8, 16, 32, 64):
                gap = gap + jnp.where(lane8 < 128 - shift, pltpu.roll(gap, 128 - shift, 1), 0.0)
            gd_out[...] = (gap + shared) * (-rate[...] / (1.0 + jnp.exp(-pre_v)))
            gk_out[...] = gk.astype(BF16)
            gq_out[...] = gq.astype(BF16)
        if step == 2:
            for o in range(1, NX):
                arrived(gx_r.at[peer_x(o)], x_sem.at[1, peer_x(o)])
            gh_out[...] = (gx_r[0] + gx_r[1] + gx_r[2] + gx_r[3]).astype(BF16)

    for pair in range(PAIRS):
        for way in range(2):
            if steps(pair, way) == 4:
                ring_step(pair, way, 4)
        last = [steps(pair, way) - 1 for way in range(2)]
        gw_out[:, cols(pair)] = part[pair, z] + ring_r[0, pair, last[0]] + ring_r[1, pair, last[1]]

    for made in sent:
        made.wait_send()


def local(hidden, value_weight, key_vecs, queries, decay_pre, decay_rate, cotangent):
    vmem = pl.BlockSpec(memory_space=pltpu.VMEM)
    dma = pltpu.SemaphoreType.DMA
    f32 = lambda *shape: pltpu.VMEM(shape, F32)
    y_box, z_box = (NY, STATE + 8, 128), (NZ, ROWS + 8, 128)
    z_back, y_back = (NZ, ROWS, 128), (NY, STATE, 128)
    outs = pl.pallas_call(
        kernel,
        out_shape=(
            jax.ShapeDtypeStruct((TOK, STATE), BF16),
            jax.ShapeDtypeStruct((TOK, STATE), BF16),
            jax.ShapeDtypeStruct((HEADS, TOK), F32),
            jax.ShapeDtypeStruct((16, 2048), BF16),
            jax.ShapeDtypeStruct((64, 512), F32),
        ),
        in_specs=[vmem] * 7,
        out_specs=[vmem] * 5,
        scratch_shapes=[
            *[f32(*y_box)] * 4,
            *[f32(*z_box)] * 4,
            *[f32(*z_back)] * 4,
            *[f32(*y_back)] * 4,
            f32(NZ, NY, 64, TOK),
            f32(NY, NZ, 64, TOK),
            pltpu.VMEM((512, 512), BF16),
            f32(PAIRS, TOK, 128),
            f32(PAIRS, NY, TOK, 128),
            f32(PAIRS, NZ, 64, 128),
            f32(2, PAIRS, 4, 64, 128),
            f32(2, PAIRS, 4, 64, 128),
            f32(NX, 2, 16, 2048),
            f32(NX, 16, 2048),
            f32(NX, 16, 2048),
            f32(NX, 16, 2048),
            f32(PAIRS, TOK, 128),
            pltpu.VMEM((TOK, 512), BF16),
            f32(HEADS, TOK),
            dma((2, 5, NY)),
            dma((2, 4, NZ)),
            dma((2, PAIRS, NY)),
            dma((2, 2, PAIRS, 4)),
            dma((2,)),
            dma((2, NX)),
        ],
        compiler_params=pltpu.CompilerParams(
            collective_id=0, has_side_effects=True, vmem_limit_bytes=48 * 1024 * 1024
        ),
        name="mixer_backward",
    )(
        hidden,
        value_weight,
        key_vecs.reshape(TOK, STATE),
        queries.reshape(TOK, STATE),
        decay_pre.T,
        jnp.broadcast_to(decay_rate[:, None], (HEADS, TOK)),
        cotangent.reshape(TOK, 512),
    )
    gk, gq, gd, gh, gw = outs
    return gk.reshape(TOK, 1, STATE), gq.reshape(TOK, 1, STATE), gd.T, gh, gw


def solution(mesh):
    split = Mesh(mesh.devices.reshape(NZ, NY, NX, 2), ("z", "y", "x", "c"))
    placed = (
        P(SP, None),
        P(None, TP),
        P(SP, TP, None),
        P(SP, TP, None),
        P(SP, TP),
        P(TP),
        P(SP, TP, None),
    )
    return jax.shard_map(
        local,
        mesh=split,
        in_specs=placed,
        out_specs=(P(SP, TP, None), P(SP, TP, None), P(SP, TP), P(SP + TP, None), P(SP, TP)),
        check_vma=False,
    )
```

time: 291 us -> 70.6 us (0.24)
  waiting for transfers between devices: 174 us -> 0 us
  Pallas kernels: 0 us -> 59.6 us
  blocking collectives: 41 us -> 0 us
  matrix products: 25.4 us -> 0 us
  other arithmetic: 21.6 us -> 0 us
  between operations: 14.5 us -> 0.66 us
  local copies, waits for them, and re-layouts: 13.9 us -> 9.67 us
    all_gather x4 -> x0, waiting for transfers between devices: 89.8 us -> none  [carried_in(): pieces = jax.tree.map(lambda part: lax.all_gather(part, axis), running)]
    pallas_call x0 -> x1, Pallas kernels: none -> 59.6 us  [local(): pl.pallas_call(kernel, out_shape=(jax.ShapeDtypeStruct((TOK, STATE), BF16...]
    reduce_scatter x2 -> x0, waiting for transfers between devices: 55.5 us -> none  [the longest x1 43.1 us: summed_rows_2(): running = lax.psum_scatter(running, axis, scatter_dimension=0, tiled=True)]
    all_gather x3 -> x0, blocking collectives: 41 us -> none  [carried_in(): pieces = jax.tree.map(lambda part: lax.all_gather(part, axis), running)]
    unnamed x8 -> x0, waiting for transfers between devices: 28.3 us -> none
    dot_general x14 -> x0, matrix products: 25.4 us -> none  [the longest x3 8.74 us: local_mixer(): jnp.einsum('thn,shn->hts', query_heads, key_heads, precision=highest)]
    reduce_sum x2 -> x0, other arithmetic: 5.77 us -> none  [the longest x1 4.39 us: local_mixer(): jnp.exp(cumulative[-1])[:, None, None] * state_in]
    mul x5 -> x0, other arithmetic: 4.22 us -> none  [the longest x1 1.54 us: local_mixer(): log_decay = -decay_rate[None, :] * jax.nn.softplus(decay_pre)]
  transfers between devices with their start and end apart: 7 -> 0, of which waited for: 7 -> 0; matrix products, arithmetic and copies ran while one was open for 14% -> 0% of each run, Pallas kernels for 0% -> 0%
where the time goes in v1:
time: 70.6 us; the launch traced here: 69.9 us
  Pallas kernels  59.6 us (84%)
  local copies, waits for them, and re-layouts  9.67 us (14%)
    pallas_call x1, Pallas kernels, local(): pl.pallas_call(kernel, out_shape=(jax.ShapeDtypeStruct((TOK, STATE), BF16...  59.6 us
    unnamed x15, local copies, waits for them, and re-layouts  7.94 us

profile of v1, /device:TPU:2, one launch (start us, length us, event | category | flops | bytes accessed | tf_op | source)
XLA Modules:
  0.0 69.9 jit_solution(3892130865592930827)
XLA Ops:
  0.6 0.7 %broadcast_in_dim.2.rate = f32[8,128]{1,0:T(8,128)S(1)} broadcast(f32[8]{0:T(128)} %param.12), dimensions={0} | broadcast | bytes 4128 | tf_op jit(solution)/shard_map/broadcast_in_dim | solution.py:403
  1.4 1.0 %copy.13.cot = bf16[128,512]{1,0:T(8,128)(2,1)S(1)} copy(bf16[128,512]{0,1:T(8,128)(2,1)} %bitcast.13) | data formatting | bytes 262144 | tf_op jit(solution)/shard_map/reshape | solution.py:404
  2.4 0.0 copy-start
  2.4 1.6 %copy-done = bf16[2048,512]{1,0:T(8,128)(2,1)S(1)} copy-done((bf16[2048,512]{1,0:T(8,128)(2,1)S(1)}, bf16[2048,512]{1,0:T(8,128)(2,1)}, u32[]{:S(2)}) %copy-start) | copy-done | bytes 2097176
  4.0 0.0 copy-start.1
  4.0 1.0 %copy-done.1 = bf16[128,2048]{1,0:T(8,128)(2,1)S(1)} copy-done((bf16[128,2048]{1,0:T(8,128)(2,1)S(1)}, bf16[128,2048]{1,0:T(8,128)(2,1)}, u32[]{:S(2)}) %copy-start.1) | copy-done | bytes 524312
  5.0 0.0 copy-start.2
  5.0 0.8 %copy-done.2 = bf16[128,1,128]{2,0,1:T(8,128)(2,1)S(1)} copy-done((bf16[128,1,128]{2,0,1:T(8,128)(2,1)S(1)}, bf16[128,1,128]{2,0,1:T(8,128)(2,1)}, u32[]{:S(2)}) %copy-start.2) | copy-done | bytes 32792
  5.8 0.0 copy-start.3
  5.8 0.8 %copy-done.3 = bf16[128,1,128]{2,0,1:T(8,128)(2,1)S(1)} copy-done((bf16[128,1,128]{2,0,1:T(8,128)(2,1)S(1)}, bf16[128,1,128]{2,0,1:T(8,128)(2,1)}, u32[]{:S(2)}) %copy-start.3) | copy-done | bytes 32792
  6.5 0.0 copy-start.4
  6.5 0.7 copy-done.4
  7.2 59.6 %mixer_backward.1 = (bf16[128,128]{1,0:T(8,128)(2,1)S(1)}, bf16[128,128]{1,0:T(8,128)(2,1)S(1)}, f32[8,128]{1,0:T(8,128)S(1)}, bf16[16,2048]{1,0:T(8,128)(2,1)S(1)}, f32[64,512]{1,0:T(8,128)S(1)}) custom-call(bf16[128,2048]{1,0:T(8,128)(2,1)S(1)} %copy-done.1, bf16[2048,512]{1,0:T(8,128)(2,1)S(1)} %copy-done, bf16[128,128]{1,0:T(8,128)(2,1)S(1)} %bitcast.7, ...), custom_call_target="tpu_custom_call" | custom-call | tf_op jit(solution)/shard_map/mixer_backward/pallas_call | solution.py:355
  66.8 0.6 copy.19
  67.4 0.6 copy.20
  68.0 0.6 copy.21
  68.6 0.6 copy.22
  69.3 0.7 copy.23
Async XLA Ops:
  2.4 1.6 %copy-start = (bf16[2048,512]{1,0:T(8,128)(2,1)S(1)}, bf16[2048,512]{1,0:T(8,128)(2,1)}, u32[]{:S(2)}) copy-start(bf16[2048,512]{1,0:T(8,128)(2,1)} %w.1) | copy-start | bytes 6291460
  4.0 1.0 %copy-start.1 = (bf16[128,2048]{1,0:T(8,128)(2,1)S(1)}, bf16[128,2048]{1,0:T(8,128)(2,1)}, u32[]{:S(2)}) copy-start(bf16[128,2048]{1,0:T(8,128)(2,1)} %hid.1) | copy-start | bytes 1572868
  5.0 0.8 %copy-start.2 = (bf16[128,1,128]{2,0,1:T(8,128)(2,1)S(1)}, bf16[128,1,128]{2,0,1:T(8,128)(2,1)}, u32[]{:S(2)}) copy-start(bf16[128,1,128]{2,0,1:T(8,128)(2,1)} %param.9) | copy-start | bytes 98308
  5.8 0.8 %copy-start.3 = (bf16[128,1,128]{2,0,1:T(8,128)(2,1)S(1)}, bf16[128,1,128]{2,0,1:T(8,128)(2,1)}, u32[]{:S(2)}) copy-start(bf16[128,1,128]{2,0,1:T(8,128)(2,1)} %param.10) | copy-start | bytes 98308
  6.5 0.7 copy-start.4

commit v2 on v1

v2 whole, which is shorter than its diff:
```python
import contextlib

import jax
import jax.numpy as jnp
from jax import lax
from jax.experimental import pallas as pl
from jax.experimental.pallas import tpu as pltpu
from jax.sharding import Mesh
from jax.sharding import PartitionSpec as P

F32, BF16 = jnp.float32, jnp.bfloat16
MESH = pl.DeviceIdType.MESH
SP, TP = ("z", "y"), ("x", "c")
NZ, NY, NX = 8, 4, 4
TOK, STATE, PAIRS, HEADS = 128, 128, 4, 8
ROWS = STATE // NZ
VMEM_LIMIT = 65 * 1024 * 1000


def dot(a, b, dims=((1,), (0,))):
    return lax.dot_general(a, b, (dims, ((), ())), preferred_element_type=F32)


def halves(a):
    high = a.astype(BF16)
    return high, (a - high.astype(F32)).astype(BF16)


def dot_fine_right(a, b, dims=((1,), (0,))):
    high, low = halves(b)
    return dot(a, high, dims) + dot(a, low, dims)


def dot_fine_left(a, b, dims=((1,), (0,))):
    high, low = halves(a)
    return dot(high, b, dims) + dot(low, b, dims)


def dot_fine(a, b, dims=((1,), (0,))):
    a_high, a_low = halves(a)
    b_high, b_low = halves(b)
    return dot(a_high, b_high, dims) + dot(a_high, b_low, dims) + dot(a_low, b_high, dims)


def cols(pair):
    return slice(128 * pair, 128 * pair + 128)


def kernel(
    hid_at, w_at, k_at, q_at, pre_at, rate_at, cot_at,
    gk_at, gq_at, gd_at, gh_at, gw_at,
    ys_b, yr_b, ys_f, yr_f, zs_b, zr_b, zs_f, zr_f,
    zbs_b, zbr_b, zbs_f, zbr_f, ybs_b, ybr_b, ybs_f, ybr_f,
    hid_t, hid_p, hid_x, hid_c, hid_all, gv_s, gv_r, part, ring_s, ring_r,
    gh_s, gh_r, gx_s, gx_r, zg_s, zg_r, k_s, k_r, cum_s, cum_r, fade, gv_own, vals, row_sum,
    gk_out, gq_out, gd_out, gh_out, gw_out,
    hid, w, k_in, q_in, pre, rate_in, cot_t, cot,
    y_sem, z_sem, ag_sem, ring_sem, d_sem, x_sem, in_sem, h_sem, out_sem, zg_sem,
):
    z, y = lax.axis_index("z"), lax.axis_index("y")
    x, c = lax.axis_index("x"), lax.axis_index("c")
    lane = lax.broadcasted_iota(jnp.int32, (128, 128), 1)
    first_head = lane[0:1, :] < 64
    sent, stored = [], []
    stack = contextlib.ExitStack()

    def phase(name):
        stack.close()
        stack.enter_context(jax.named_scope(name))

    def put(src, dst, at):
        made = pltpu.make_async_copy(src, dst, out_sem.at[at])
        made.start()
        stored.append(made)

    def peer_y(o):
        return lax.rem(y + o, NY)

    def peer_z(o):
        return lax.rem(z + o, NZ)

    def peer_x(o):
        return lax.rem(x + o, NX)

    def copy(src, dst, s_sem, r_sem, **where):
        return pltpu.make_async_remote_copy(
            src_ref=src, dst_ref=dst, send_sem=s_sem, recv_sem=r_sem, device_id=where, device_id_type=MESH
        )

    def send(src, dst, s_sem, r_sem, **where):
        made = copy(src, dst, s_sem, r_sem, **where)
        made.start()
        sent.append(made)

    def arrived(dst, r_sem):
        copy(dst, dst, r_sem, r_sem, c=1 - c).wait_recv()

    def send_y(kind, src, dst):
        for o in range(1, NY):
            send(src.at[peer_y(o)], dst.at[y], y_sem.at[0, kind, peer_y(o)], y_sem.at[1, kind, y], y=peer_y(o))

    def share_y(kind, src, dst):
        for o in range(1, NY):
            send(src, dst.at[y], y_sem.at[0, kind, peer_y(o)], y_sem.at[1, kind, y], y=peer_y(o))

    def wait_y(kind, dst):
        for o in range(1, NY):
            arrived(dst.at[peer_y(o)], y_sem.at[1, kind, peer_y(o)])

    def send_z(kind, src, dst):
        for o in range(1, NZ):
            send(src.at[peer_z(o)], dst.at[z], z_sem.at[0, kind, peer_z(o)], z_sem.at[1, kind, z], z=peer_z(o))

    def wait_z(kind, dst):
        for o in range(1, NZ):
            arrived(dst.at[peer_z(o)], z_sem.at[1, kind, peer_z(o)])

    phase("enter")
    loads = [
        pltpu.make_async_copy(src, dst, in_sem.at[i])
        for i, (src, dst) in enumerate(
            [(pre_at, pre), (rate_at, rate_in), (cot_at, cot_t), (q_at, q_in), (k_at, k_in), (hid_at, hid), (w_at, w)]
        )
    ]
    for made in loads:
        made.start()

    barrier = pltpu.get_barrier_semaphore()
    for o in range(1, NY):
        pl.semaphore_signal(barrier, inc=1, device_id={"y": peer_y(o)}, device_id_type=MESH)
    for o in range(1, NZ):
        pl.semaphore_signal(barrier, inc=1, device_id={"z": peer_z(o)}, device_id_type=MESH)
    for o in range(1, NX):
        pl.semaphore_signal(barrier, inc=1, device_id={"x": peer_x(o)}, device_id_type=MESH)
    pl.semaphore_signal(barrier, inc=1, device_id={"c": 1 - c}, device_id_type=MESH)

    phase("decay")
    loads[0].wait()
    loads[1].wait()
    pre_v = pre[...]
    square = lax.broadcasted_iota(jnp.int32, (8, 8), 0) == lax.broadcasted_iota(jnp.int32, (8, 8), 1)
    rate = jnp.sum(jnp.where(square, jnp.broadcast_to(rate_in[...], (8, 8)), 0.0), axis=1, keepdims=True)
    soft = jnp.maximum(pre_v, 0.0) + jnp.log1p(jnp.exp(-jnp.abs(pre_v)))
    cum = -rate * soft
    lane8 = lane[0:8, :]
    for shift in (1, 2, 4, 8, 16, 32, 64):
        cum = cum + jnp.where(lane8 >= shift, pltpu.roll(cum, shift, 1), 0.0)
    cum_s[...] = cum
    cum_r[y] = cum
    total = jnp.broadcast_to(cum[:, 127:128], (8, 128))
    factor = jnp.exp(total)
    cum_t = cum.T
    from_start = jnp.exp(cum)
    from_start_t = from_start.T
    to_end_t = jnp.exp(total - cum).T

    def spread(columns, pair):
        return jnp.where(first_head, columns[:, 2 * pair : 2 * pair + 1], columns[:, 2 * pair + 1 : 2 * pair + 2])

    def row_of(gains, pair):
        return jnp.where(first_head, gains[2 * pair : 2 * pair + 1, :], gains[2 * pair + 1 : 2 * pair + 2, :])

    phase("pull")
    loads[2].wait()
    loads[3].wait()
    q = q_in[...]
    q_t = q.astype(F32).T.astype(BF16)
    upper = lax.broadcasted_iota(jnp.int32, (128, 128), 0) < 64
    for pair in range(PAIRS):
        growth = jnp.where(upper, from_start[2 * pair : 2 * pair + 1, :], from_start[2 * pair + 1 : 2 * pair + 2, :])
        scaled = growth * cot_t[cols(pair), :].astype(F32)
        ys_b[pair, 0:128, :] = dot_fine_right(q_t, scaled, ((1,), (1,)))
        ys_b[pair, 128:136, :] = jnp.broadcast_to(row_of(factor, pair), (8, 128))
    yr_b[y] = ys_b[y]
    loads[4].wait()
    k = k_in[...]
    k_s[...] = k.astype(F32)
    k_r[y] = k_s[...]

    phase("barrier")
    pl.semaphore_wait(barrier, NY + NZ + NX - 2)
    send_y(0, ys_b, yr_b)

    phase("hidden")
    loads[5].wait()
    for block in range(16):
        turned = hid[:, cols(block)].astype(F32).T
        hid_t[block // 2, 2 * (block % 2) : 2 * (block % 2) + 2] = turned.reshape(2, 64, 128)
    seat = 2 * x + c
    for o in range(1, NY):
        send(hid_t.at[seat, peer_y(o)], hid_p.at[y], y_sem.at[0, 2, peer_y(o)], y_sem.at[1, 2, y], y=peer_y(o))
    hid_p[y] = hid_t[seat, y]
    share_y(5, k_s, k_r)
    share_y(6, cum_s, cum_r)

    phase("values")
    loads[6].wait()
    k_t = k_s[...].T.astype(BF16)
    for half in range(2):
        span = slice(256 * half, 256 * half + 256)
        vals[:, span] = dot(hid[...], w[:, span]).astype(BF16)
    for pair in range(PAIRS):
        scaled = spread(to_end_t, pair) * vals[:, cols(pair)].astype(F32)
        ys_f[pair, 0:128, :] = dot_fine_right(k_t, scaled)
        ys_f[pair, 128:136, :] = jnp.broadcast_to(row_of(factor, pair), (8, 128))
    yr_f[y] = ys_f[y]

    phase("block")
    for pair in range(PAIRS):
        cot[:, cols(pair)] = cot_t[cols(pair), :].astype(F32).T.astype(BF16)
    score = dot(k, q, ((1,), (1,)))
    causal = lax.broadcasted_iota(jnp.int32, (128, 128), 0) <= lane
    blend = jnp.zeros((128, 128), F32)
    for pair in range(PAIRS):
        cot_pair, val_pair = cot[:, cols(pair)], vals[:, cols(pair)]
        inner = jnp.zeros((128, 128), F32)
        for side in range(2):
            head = 2 * pair + side
            mine = first_head if side == 0 else jnp.logical_not(first_head)
            across = jnp.where(causal, cum[head : head + 1, :] - cum_t[:, head : head + 1], 0.0)
            damping = jnp.where(causal, jnp.exp(across), 0.0)
            weight = score * damping
            cot_head = jnp.where(mine, cot_pair.astype(F32), 0.0).astype(BF16)
            inner = inner + dot_fine_left(weight, cot_head)
            moved = dot(val_pair, cot_head, ((1,), (1,)))
            blend = blend + moved * damping
            row_sum[head : head + 1, :] = jnp.sum(moved * weight, axis=0, keepdims=True)
        gv_s[pair] = inner

    def scan_plane(got, kept, z_send, reverse):
        state, gain = None, None
        order = range(NY - 1, -1, -1) if reverse else range(NY)
        for block in order:
            value, here = got[block, 0:128, :], got[block, 128:129, :]
            if state is None:
                kept[block] = jnp.zeros((128, 128), F32)
                state, gain = value, here
            else:
                kept[block] = state
                state, gain = here * state + value, gain * here
        for row in range(NZ):
            z_send[row, 0:ROWS, :] = state[row * ROWS : row * ROWS + ROWS, :]
            z_send[row, ROWS : ROWS + 8, :] = jnp.broadcast_to(gain, (8, 128))

    def scan_z(got, back, reverse):
        state = None
        for plane in range(NZ - 1, -1, -1) if reverse else range(NZ):
            value, here = got[plane, 0:ROWS, :], got[plane, ROWS : ROWS + 1, :]
            if state is None:
                back[plane] = jnp.zeros((ROWS, 128), F32)
                state = value
            else:
                back[plane] = state
                state = here * state + value

    def finish_plane(got, kept, plane_in, reverse):
        incoming = plane_in[...].reshape(STATE, 128)
        gain = None
        for block in range(NY - 1, -1, -1) if reverse else range(NY):
            kept[block] = kept[block] + (incoming if gain is None else gain * incoming)
            here = got[block, 128:129, :]
            gain = here if gain is None else gain * here

    phase("scan_y_b")
    wait_y(0, yr_b)
    scan_plane(yr_b, ybs_b, zs_b, True)
    zr_b[z] = zs_b[z]
    send_z(0, zs_b, zr_b)
    ybr_b[y] = ybs_b[y]
    send_y(3, ybs_b, ybr_b)
    send_y(1, ys_f, yr_f)

    phase("hidden_x")
    wait_y(2, hid_p)
    for o in range(1, NX):
        send(hid_p, hid_x.at[x], h_sem.at[0, peer_x(o)], h_sem.at[1, x], x=peer_x(o))
    hid_x[x] = hid_p[...]

    phase("scan_z_b")
    wait_z(0, zr_b)
    scan_z(zr_b, zbs_b, True)
    zbr_b[z] = zbs_b[z]
    send_z(2, zbs_b, zbr_b)

    phase("wait_suffix")
    wait_y(3, ybr_b)
    phase("gv_plane")
    for pair in range(PAIRS):
        gv_s[pair] = gv_s[pair] + spread(to_end_t, pair) * dot_fine_right(k, ybr_b[pair])
    for slot in range(PAIRS):
        for o in range(1, NY):
            send(
                gv_s.at[peer_y(o + slot)], gv_r.at[slot, y], ag_sem.at[0, slot, peer_y(o)], ag_sem.at[1, slot, y],
                y=peer_y(o),
            )
        gv_r[slot, y] = gv_s[peer_y(slot)]

    phase("scan_y_f")
    wait_y(1, yr_f)
    scan_plane(yr_f, ybs_f, zs_f, False)
    zr_f[z] = zs_f[z]
    send_z(1, zs_f, zr_f)

    phase("hidden_c")
    for o in range(1, NX):
        arrived(hid_x.at[peer_x(o)], h_sem.at[1, peer_x(o)])
    send(hid_x, hid_c, d_sem.at[0, 1], d_sem.at[1, 1], c=1 - c)

    phase("fade")
    wait_y(5, k_r)
    wait_y(6, cum_r)
    tail = jnp.zeros((8, 1), F32)
    tail_own = jnp.zeros((8, 1), F32)
    for block in range(NY - 1, -1, -1):
        here = cum_r[block]
        tail_own = jnp.where(y == block, tail, tail_own)
        tail = tail + here[:, 127:128]
        fade_t = jnp.exp(tail - here).T
        for pair in range(PAIRS):
            fade[block, pair] = spread(fade_t, pair)
    gain_own = jnp.exp(jnp.broadcast_to(tail_own, (8, 128)))
    k_all = k_r[...].reshape(512, 128).astype(BF16)
    arrived(hid_c, d_sem.at[1, 1])
    for across_x in range(NX):
        for block in range(NY):
            hid_all[across_x, c, :, cols(block)] = hid_x[across_x, block].astype(BF16)
            hid_all[across_x, 1 - c, :, cols(block)] = hid_c[across_x, block].astype(BF16)

    phase("wait_zg")
    wait_z(2, zbr_b)
    zg_s[...] = zbr_b[...].reshape(STATE, 128)
    zg_r[0] = zg_s[...]
    for o in range(1, NY):
        send(zg_s, zg_r.at[NY - o], zg_sem.at[0, NY - o], zg_sem.at[1, NY - o], y=peer_y(o))

    def steps(slot, way):
        return 4 if (slot + way) % 2 == 0 else 3

    def ring_target(slot, way, step):
        n = steps(slot, way)
        return peer_z(n - step) if way == 0 else peer_z(NZ - n + step)

    def ring_send(src, slot, way, step):
        send(
            src, ring_r.at[way, slot, step], ring_sem.at[0, way, slot, step], ring_sem.at[1, way, slot, step],
            z=peer_z(1) if way == 0 else peer_z(NZ - 1),
        )

    def ring_step(slot, way, step):
        if not 1 <= step <= steps(slot, way):
            return
        arrived(ring_r.at[way, slot, step - 1], ring_sem.at[1, way, slot, step - 1])
        if step < steps(slot, way):
            ring_s[way, slot, step] = ring_r[way, slot, step - 1] + part[slot, ring_target(slot, way, step)]
            ring_send(ring_s.at[way, slot, step], slot, way, step)

    def weight_slot(slot):
        pair = peer_y(slot)
        if slot > 0:
            arrived(zg_r.at[slot], zg_sem.at[1, slot])
        for o in range(1, NY):
            arrived(gv_r.at[slot, peer_y(o)], ag_sem.at[1, slot, peer_y(o)])
        phase(f"weight{slot}")
        fresh = dot_fine_right(k_all, zg_r[slot])
        for block in range(NY):
            gv_r[slot, block] = gv_r[slot, block] + fade[block, pair] * fresh[128 * block : 128 * block + 128, :]
        gv_own[pair] = gv_r[slot, y]
        gathered = gv_r[slot].reshape(512, 128).astype(BF16)
        part[slot] = dot(hid_all[...].reshape(512, 512), gathered).reshape(NZ, 64, 128)
        for way in range(2):
            ring_send(part.at[slot, ring_target(slot, way, 0)], slot, way, 0)

    phase("wait_ag0")
    weight_slot(0)

    phase("scan_z_f")
    wait_z(1, zr_f)
    scan_z(zr_f, zbs_f, False)
    zbr_f[z] = zbs_f[z]
    send_z(3, zbs_f, zbr_f)

    phase("ring0_1")
    for way in range(2):
        ring_step(0, way, 1)

    phase("back_y_f")
    wait_z(3, zbr_f)
    finish_plane(yr_f, ybs_f, zbr_f, False)
    ybr_f[y] = ybs_f[y]
    send_y(4, ybs_f, ybr_f)

    phase("ring0_2")
    for way in range(2):
        ring_step(0, way, 2)

    for slot in range(1, PAIRS):
        phase(f"wait_ag{slot}")
        weight_slot(slot)

    phase("grad_h")
    grad_v = jnp.concatenate([gv_own[pair].astype(BF16) for pair in range(PAIRS)], axis=1)
    for part_now in range(4):
        span = slice(512 * part_now, 512 * part_now + 512)
        gh_s[:, :, :, span] = dot(grad_v, w[span, :], ((1,), (1,))).reshape(NX, 2, 16, 512)
    send(gh_s.at[:, 1 - c], gh_r, d_sem.at[0, 0], d_sem.at[1, 0], c=1 - c)

    def ring_turn(step):
        phase(f"ring{step}")
        for slot in range(PAIRS):
            for way in range(2):
                ring_step(slot, way, step + 2 if slot == 0 else step)

    ring_turn(1)
    phase("chip_pair")
    arrived(gh_r, d_sem.at[1, 0])
    gx_s[...] = gh_s[:, c] + gh_r[...]
    for o in range(1, NX):
        send(gx_s.at[peer_x(o)], gx_r.at[x], x_sem.at[0, peer_x(o)], x_sem.at[1, x], x=peer_x(o))
    gx_r[x] = gx_s[x]
    ring_turn(2)

    phase("grad_kq")
    wait_y(4, ybr_f)
    gk = dot_fine_left(blend, q)
    gq = dot_fine_left(blend.T, k)
    gap = jnp.zeros((8, 128), F32)
    shared = jnp.zeros((8, 128), F32)
    head_row = lax.broadcasted_iota(jnp.int32, (8, 128), 0)
    for pair in range(PAIRS):
        carry = ybr_f[pair]
        pull = ybr_b[pair] + row_of(gain_own, pair) * zg_r[lax.rem(pair + NY - y, NY)]
        cot_f = cot[:, cols(pair)].astype(F32)
        val_f = vals[:, cols(pair)].astype(F32)
        cot_scaled = spread(from_start_t, pair) * cot_f
        val_scaled = spread(to_end_t, pair) * val_f
        gq = gq + dot_fine(cot_scaled, carry, ((1,), (1,)))
        gk = gk + dot_fine(val_scaled, pull, ((1,), (1,)))
        out_carried = dot_fine_right(q, carry)
        from_state = dot_fine_right(k, pull)
        owner = head_row == 2 * pair + (lane8 >= 64).astype(jnp.int32)
        chooser = jnp.where(owner, 1.0, 0.0)
        change = cot_scaled * out_carried - val_f * gv_own[pair]
        gap = gap + lax.dot_general(
            chooser, change, (((1,), (1,)), ((), ())),
            precision=lax.Precision.HIGHEST, preferred_element_type=F32,
        )
        whole = jnp.sum(val_scaled * from_state, axis=0, keepdims=True)
        whole = whole + row_of(factor, pair) * jnp.sum(carry * pull, axis=0, keepdims=True)
        shared = shared + jnp.sum(chooser * whole, axis=1, keepdims=True)
    gap = gap + row_sum[...]
    for shift in (1, 2, 4, 8, 16, 32, 64):
        gap = gap + jnp.where(lane8 < 128 - shift, pltpu.roll(gap, 128 - shift, 1), 0.0)
    gd_out[...] = (gap + shared) * (-rate / (1.0 + jnp.exp(-pre_v)))
    gk_out[...] = gk.astype(BF16)
    gq_out[...] = gq.astype(BF16)
    put(gk_out, gk_at, 0)
    put(gq_out, gq_at, 1)
    put(gd_out, gd_at, 2)

    ring_turn(3)
    phase("out_h")
    for o in range(1, NX):
        arrived(gx_r.at[peer_x(o)], x_sem.at[1, peer_x(o)])
    gh_out[...] = (gx_r[0] + gx_r[1] + gx_r[2] + gx_r[3]).astype(BF16)
    put(gh_out, gh_at, 3)

    ring_turn(4)
    for slot in range(PAIRS):
        last = [steps(slot, way) - 1 for way in range(2)]
        gw_out[slot] = part[slot, z] + ring_r[0, slot, last[0]] + ring_r[1, slot, last[1]]
        put(gw_out.at[slot], gw_at.at[:, pl.ds(pl.multiple_of(128 * peer_y(slot), 128), 128)], 4 + slot)

    phase("drain")
    for made in sent:
        made.wait_send()
    for made in stored:
        made.wait()
    stack.close()


def store_all(*refs):
    sems = refs[15]
    taken = [pltpu.make_async_copy(refs[i], refs[10 + i], sems.at[0, i]) for i in range(5)]
    given = [pltpu.make_async_copy(refs[10 + i], refs[5 + i], sems.at[1, i]) for i in range(5)]
    for made in taken:
        made.start()
    for take, give in zip(taken, given):
        take.wait()
        give.start()
    for made in given:
        made.wait()


def local(hidden, value_weight, key_vecs, queries, decay_pre, decay_rate, cotangent):
    dma = pltpu.SemaphoreType.DMA
    f32 = lambda *shape: pltpu.VMEM(shape, F32)
    y_box, z_box = (NY, STATE + 8, 128), (NZ, ROWS + 8, 128)
    z_back, y_back = (NZ, ROWS, 128), (NY, STATE, 128)
    outs = pl.pallas_call(
        kernel,
        out_shape=(
            jax.ShapeDtypeStruct((TOK, STATE), BF16),
            jax.ShapeDtypeStruct((TOK, STATE), BF16),
            jax.ShapeDtypeStruct((HEADS, TOK), F32),
            jax.ShapeDtypeStruct((16, 2048), BF16),
            jax.ShapeDtypeStruct((64, 512), F32),
        ),
        in_specs=[pl.BlockSpec(memory_space=pl.ANY)] * 7,
        out_specs=[pl.BlockSpec(memory_space=pl.ANY)] * 5,
        scratch_shapes=[
            *[f32(*y_box)] * 4,
            *[f32(*z_box)] * 4,
            *[f32(*z_back)] * 4,
            *[f32(*y_back)] * 4,
            f32(NZ, NY, 64, TOK),
            f32(NY, 64, TOK),
            f32(NX, NY, 64, TOK),
            f32(NX, NY, 64, TOK),
            pltpu.VMEM((NX, 2, 64, 512), BF16),
            f32(PAIRS, TOK, 128),
            f32(PAIRS, NY, TOK, 128),
            f32(PAIRS, NZ, 64, 128),
            f32(2, PAIRS, 4, 64, 128),
            f32(2, PAIRS, 4, 64, 128),
            f32(NX, 2, 16, 2048),
            f32(NX, 16, 2048),
            f32(NX, 16, 2048),
            f32(NX, 16, 2048),
            f32(STATE, 128),
            f32(NY, STATE, 128),
            f32(TOK, STATE),
            f32(NY, TOK, STATE),
            f32(HEADS, TOK),
            f32(NY, HEADS, TOK),
            f32(NY, PAIRS, TOK, 128),
            f32(PAIRS, TOK, 128),
            pltpu.VMEM((TOK, 512), BF16),
            f32(HEADS, TOK),
            pltpu.VMEM((TOK, STATE), BF16),
            pltpu.VMEM((TOK, STATE), BF16),
            f32(HEADS, TOK),
            pltpu.VMEM((16, 2048), BF16),
            f32(PAIRS, 64, 128),
            pltpu.VMEM((TOK, 2048), BF16),
            pltpu.VMEM((2048, 512), BF16),
            pltpu.VMEM((TOK, STATE), BF16),
            pltpu.VMEM((TOK, STATE), BF16),
            f32(HEADS, TOK),
            f32(1, HEADS),
            pltpu.VMEM((512, TOK), BF16),
            pltpu.VMEM((TOK, 512), BF16),
            dma((2, 7, NY)),
            dma((2, 4, NZ)),
            dma((2, PAIRS, NY)),
            dma((2, 2, PAIRS, 4)),
            dma((2, 2)),
            dma((2, NX)),
            dma((7,)),
            dma((2, NX)),
            dma((8,)),
            dma((2, NY)),
        ],
        compiler_params=pltpu.CompilerParams(
            collective_id=0, has_side_effects=True, vmem_limit_bytes=VMEM_LIMIT
        ),
        name="mixer_backward",
    )(
        hidden,
        value_weight,
        key_vecs.reshape(TOK, STATE),
        queries.reshape(TOK, STATE),
        decay_pre.T,
        decay_rate[None, :],
        cotangent.reshape(TOK, 512).T,
    )
    gk, gq, gd, gh, gw = pl.pallas_call(
        store_all,
        out_shape=tuple(jax.ShapeDtypeStruct(o.shape, o.dtype) for o in outs),
        in_specs=[pl.BlockSpec(memory_space=pl.ANY)] * 5,
        out_specs=[pl.BlockSpec(memory_space=pl.ANY)] * 5,
        scratch_shapes=[*[pltpu.VMEM(o.shape, o.dtype) for o in outs], dma((2, 5))],
        compiler_params=pltpu.CompilerParams(vmem_limit_bytes=VMEM_LIMIT),
        name="store_all",
    )(*outs)
    return gk.reshape(TOK, 1, STATE), gq.reshape(TOK, 1, STATE), gd.T, gh, gw


def solution(mesh):
    split = Mesh(mesh.devices.reshape(NZ, NY, NX, 2), ("z", "y", "x", "c"))
    placed = (
        P(SP, None),
        P(None, TP),
        P(SP, TP, None),
        P(SP, TP, None),
        P(SP, TP),
        P(TP),
        P(SP, TP, None),
    )
    return jax.shard_map(
        local,
        mesh=split,
        in_specs=placed,
        out_specs=(P(SP, TP, None), P(SP, TP, None), P(SP, TP), P(SP + TP, None), P(SP, TP)),
        check_vma=False,
    )
```

time: 70.6 us -> 58.6 us (0.83)
  local copies, waits for them, and re-layouts: 9.67 us -> 0 us
  Pallas kernels: 59.6 us -> 57.6 us
    unnamed x15 -> x0, local copies, waits for them, and re-layouts: 7.94 us -> none
    pallas_call x1, Pallas kernels: 59.6 us -> 55.9 us  [local(): pl.pallas_call(kernel, out_shape=(jax.ShapeDtypeStruct((TOK, STATE), BF16...]
    pallas_call x0 -> x1, Pallas kernels: none -> 1.72 us  [local(): pl.pallas_call(store_all, out_shape=tuple((jax.ShapeDtypeStruct(o.shape,...]
    reshape x1 -> x0, local copies, waits for them, and re-layouts: 1 us -> none  [local(): cotangent.reshape(TOK, 512)]
    broadcast_in_dim x1 -> x0, local copies, waits for them, and re-layouts: 0.72 us -> none  [local(): jnp.broadcast_to(decay_rate[:, None], (HEADS, TOK))]
where the time goes in v2:
time: 58.6 us; the launch traced here: 58.3 us
  Pallas kernels  57.6 us (98%)
  between operations  0.64 us (1%)
    pallas_call x1, Pallas kernels, local(): pl.pallas_call(kernel, out_shape=(jax.ShapeDtypeStruct((TOK, STATE), BF16...  55.9 us
    pallas_call x1, Pallas kernels, local(): pl.pallas_call(store_all, out_shape=tuple((jax.ShapeDtypeStruct(o.shape,...  1.72 us

profile of v2, /device:TPU:2, one launch (start us, length us, event | category | flops | bytes accessed | tf_op | source)
XLA Modules:
  0.0 58.3 jit_solution(15888507797167115091)
XLA Ops:
  0.6 55.9 %mixer_backward.1 = (bf16[128,128]{1,0:T(8,128)(2,1)}, bf16[128,128]{1,0:T(8,128)(2,1)}, f32[8,128]{1,0:T(8,128)}, bf16[16,2048]{1,0:T(8,128)(2,1)}, f32[64,512]{1,0:T(8,128)}) custom-call(bf16[128,2048]{1,0:T(8,128)(2,1)} %hid_at.1, bf16[2048,512]{1,0:T(8,128)(2,1)} %w_at.1, bf16[128,128]{1,0:T(8,128)(2,1)} %bitcast.11, bf16[128,128]{1,0:T(8,128)(2,1)} %bitcast.12, ...), custom_call_target="tpu_custom_call" | custom-call | tf_op jit(solution)/shard_map/mixer_backward/pallas_call | solution.py:499
  56.6 1.7 %store_all.1 = (bf16[128,128]{1,0:T(8,128)(2,1)}, bf16[128,128]{1,0:T(8,128)(2,1)}, f32[8,128]{1,0:T(8,128)}, bf16[16,2048]{1,0:T(8,128)(2,1)}, f32[64,512]{1,0:T(8,128)}) custom-call(bf16[128,128]{1,0:T(8,128)(2,1)} %get-tuple-element.15.refs_0_, bf16[128,128]{1,0:T(8,128)(2,1)} %get-tuple-element.16.refs_1_, f32[8,128]{1,0:T(8,128)} %get-tuple-element.17.refs_2_, ...), custom_call_target="tpu_custom_call" | custom-call | tf_op jit(solution)/shard_map/store_all/pallas_call | solution.py:576

commit v3 on v2

--- a/solution.py
+++ b/solution.py
@@ -14,7 +14,7 @@
 NZ, NY, NX = 8, 4, 4
 TOK, STATE, PAIRS, HEADS = 128, 128, 4, 8
 ROWS = STATE // NZ
-VMEM_LIMIT = 65 * 1024 * 1000
+VMEM_LIMIT = 48 * 1024 * 1024
 
 
 def dot(a, b, dims=((1,), (0,))):
@@ -48,30 +48,24 @@
 
 def kernel(
     hid_at, w_at, k_at, q_at, pre_at, rate_at, cot_at,
-    gk_at, gq_at, gd_at, gh_at, gw_at,
+    gk_out, gq_out, gd_out, gh_out, gw_out,
     ys_b, yr_b, ys_f, yr_f, zs_b, zr_b, zs_f, zr_f,
     zbs_b, zbr_b, zbs_f, zbr_f, ybs_b, ybr_b, ybs_f, ybr_f,
     hid_t, hid_p, hid_x, hid_c, hid_all, gv_s, gv_r, part, ring_s, ring_r,
     gh_s, gh_r, gx_s, gx_r, zg_s, zg_r, k_s, k_r, cum_s, cum_r, fade, gv_own, vals, row_sum,
-    gk_out, gq_out, gd_out, gh_out, gw_out,
     hid, w, k_in, q_in, pre, rate_in, cot_t, cot,
-    y_sem, z_sem, ag_sem, ring_sem, d_sem, x_sem, in_sem, h_sem, out_sem, zg_sem,
+    y_sem, z_sem, ag_sem, ring_sem, d_sem, x_sem, in_sem, h_sem, zg_sem,
 ):
     z, y = lax.axis_index("z"), lax.axis_index("y")
     x, c = lax.axis_index("x"), lax.axis_index("c")
     lane = lax.broadcasted_iota(jnp.int32, (128, 128), 1)
     first_head = lane[0:1, :] < 64
-    sent, stored = [], []
+    sent = []
     stack = contextlib.ExitStack()
 
     def phase(name):
         stack.close()
         stack.enter_context(jax.named_scope(name))
-
-    def put(src, dst, at):
-        made = pltpu.make_async_copy(src, dst, out_sem.at[at])
-        made.start()
-        stored.append(made)
 
     def peer_y(o):
         return lax.rem(y + o, NY)
@@ -88,32 +82,34 @@
         )
 
     def send(src, dst, s_sem, r_sem, **where):
-        made = copy(src, dst, s_sem, r_sem, **where)
-        made.start()
-        sent.append(made)
+        copy(src, dst, s_sem, r_sem, **where).start()
 
     def arrived(dst, r_sem):
         copy(dst, dst, r_sem, r_sem, c=1 - c).wait_recv()
 
+    def drain_later(like, s_sem):
+        sent.append(copy(like, like, s_sem, s_sem, c=1 - c))
+
     def send_y(kind, src, dst):
         for o in range(1, NY):
-            send(src.at[peer_y(o)], dst.at[y], y_sem.at[0, kind, peer_y(o)], y_sem.at[1, kind, y], y=peer_y(o))
+            send(src.at[peer_y(o)], dst.at[y], y_sem.at[0, kind], y_sem.at[1, kind], y=peer_y(o))
+        drain_later(dst.at[0 : NY - 1], y_sem.at[0, kind])
 
     def share_y(kind, src, dst):
         for o in range(1, NY):
-            send(src, dst.at[y], y_sem.at[0, kind, peer_y(o)], y_sem.at[1, kind, y], y=peer_y(o))
+            send(src, dst.at[y], y_sem.at[0, kind], y_sem.at[1, kind], y=peer_y(o))
+        drain_later(dst.at[0 : NY - 1], y_sem.at[0, kind])
 
     def wait_y(kind, dst):
-        for o in range(1, NY):
-            arrived(dst.at[peer_y(o)], y_sem.at[1, kind, peer_y(o)])
+        arrived(dst.at[0 : NY - 1], y_sem.at[1, kind])
 
     def send_z(kind, src, dst):
         for o in range(1, NZ):
-            send(src.at[peer_z(o)], dst.at[z], z_sem.at[0, kind, peer_z(o)], z_sem.at[1, kind, z], z=peer_z(o))
+            send(src.at[peer_z(o)], dst.at[z], z_sem.at[0, kind], z_sem.at[1, kind], z=peer_z(o))
+        drain_later(dst.at[0 : NZ - 1], z_sem.at[0, kind])
 
     def wait_z(kind, dst):
-        for o in range(1, NZ):
-            arrived(dst.at[peer_z(o)], z_sem.at[1, kind, peer_z(o)])
+        arrived(dst.at[0 : NZ - 1], z_sem.at[1, kind])
 
     phase("enter")
     loads = [
@@ -188,7 +184,8 @@
         hid_t[block // 2, 2 * (block % 2) : 2 * (block % 2) + 2] = turned.reshape(2, 64, 128)
     seat = 2 * x + c
     for o in range(1, NY):
-        send(hid_t.at[seat, peer_y(o)], hid_p.at[y], y_sem.at[0, 2, peer_y(o)], y_sem.at[1, 2, y], y=peer_y(o))
+        send(hid_t.at[seat, peer_y(o)], hid_p.at[y], y_sem.at[0, 2], y_sem.at[1, 2], y=peer_y(o))
+    drain_later(hid_p.at[0 : NY - 1], y_sem.at[0, 2])
     hid_p[y] = hid_t[seat, y]
     share_y(5, k_s, k_r)
     share_y(6, cum_s, cum_r)
@@ -273,7 +270,8 @@
     phase("hidden_x")
     wait_y(2, hid_p)
     for o in range(1, NX):
-        send(hid_p, hid_x.at[x], h_sem.at[0, peer_x(o)], h_sem.at[1, x], x=peer_x(o))
+        send(hid_p, hid_x.at[x], h_sem.at[0], h_sem.at[1], x=peer_x(o))
+    drain_later(hid_x.at[0 : NX - 1], h_sem.at[0])
     hid_x[x] = hid_p[...]
 
     phase("scan_z_b")
@@ -287,24 +285,15 @@
     phase("gv_plane")
     for pair in range(PAIRS):
         gv_s[pair] = gv_s[pair] + spread(to_end_t, pair) * dot_fine_right(k, ybr_b[pair])
-    for slot in range(PAIRS):
+
+    def share_slot(slot):
         for o in range(1, NY):
-            send(
-                gv_s.at[peer_y(o + slot)], gv_r.at[slot, y], ag_sem.at[0, slot, peer_y(o)], ag_sem.at[1, slot, y],
-                y=peer_y(o),
-            )
+            send(gv_s.at[peer_y(o + slot)], gv_r.at[slot, y], ag_sem.at[0, slot], ag_sem.at[1, slot], y=peer_y(o))
+        drain_later(gv_r.at[slot, 0 : NY - 1], ag_sem.at[0, slot])
         gv_r[slot, y] = gv_s[peer_y(slot)]
 
-    phase("scan_y_f")
-    wait_y(1, yr_f)
-    scan_plane(yr_f, ybs_f, zs_f, False)
-    zr_f[z] = zs_f[z]
-    send_z(1, zs_f, zr_f)
-
-    phase("hidden_c")
-    for o in range(1, NX):
-        arrived(hid_x.at[peer_x(o)], h_sem.at[1, peer_x(o)])
-    send(hid_x, hid_c, d_sem.at[0, 1], d_sem.at[1, 1], c=1 - c)
+    share_slot(0)
+    share_slot(1)
 
     phase("fade")
     wait_y(5, k_r)
@@ -320,19 +309,35 @@
             fade[block, pair] = spread(fade_t, pair)
     gain_own = jnp.exp(jnp.broadcast_to(tail_own, (8, 128)))
     k_all = k_r[...].reshape(512, 128).astype(BF16)
+
+    phase("hidden_c")
+    arrived(hid_x.at[0 : NX - 1], h_sem.at[1])
+    send(hid_x, hid_c, d_sem.at[0, 1], d_sem.at[1, 1], c=1 - c)
+    drain_later(hid_x, d_sem.at[0, 1])
+
+    phase("wait_zg")
+    wait_z(2, zbr_b)
+    zg_s[...] = zbr_b[...].reshape(STATE, 128)
+    zg_r[0] = zg_s[...]
+    for o in range(1, NY):
+        send(zg_s, zg_r.at[NY - o], zg_sem.at[0], zg_sem.at[1], y=peer_y(o))
+    drain_later(zg_r.at[0 : NY - 1], zg_sem.at[0])
+    share_slot(2)
+    share_slot(3)
+
+    phase("scan_y_f")
+    wait_y(1, yr_f)
+    scan_plane(yr_f, ybs_f, zs_f, False)
+    zr_f[z] = zs_f[z]
+    send_z(1, zs_f, zr_f)
+
+    phase("hid_all")
     arrived(hid_c, d_sem.at[1, 1])
     for across_x in range(NX):
         for block in range(NY):
             hid_all[across_x, c, :, cols(block)] = hid_x[across_x, block].astype(BF16)
             hid_all[across_x, 1 - c, :, cols(block)] = hid_c[across_x, block].astype(BF16)
 
-    phase("wait_zg")
-    wait_z(2, zbr_b)
-    zg_s[...] = zbr_b[...].reshape(STATE, 128)
-    zg_r[0] = zg_s[...]
-    for o in range(1, NY):
-        send(zg_s, zg_r.at[NY - o], zg_sem.at[0, NY - o], zg_sem.at[1, NY - o], y=peer_y(o))
-
     def steps(slot, way):
         return 4 if (slot + way) % 2 == 0 else 3
 
@@ -342,46 +347,70 @@
 
     def ring_send(src, slot, way, step):
         send(
-            src, ring_r.at[way, slot, step], ring_sem.at[0, way, slot, step], ring_sem.at[1, way, slot, step],
+            src, ring_r.at[way, slot, step], ring_sem.at[PAIRS, 0], ring_sem.at[slot, step],
             z=peer_z(1) if way == 0 else peer_z(NZ - 1),
         )
 
-    def ring_step(slot, way, step):
-        if not 1 <= step <= steps(slot, way):
-            return
-        arrived(ring_r.at[way, slot, step - 1], ring_sem.at[1, way, slot, step - 1])
-        if step < steps(slot, way):
-            ring_s[way, slot, step] = ring_r[way, slot, step - 1] + part[slot, ring_target(slot, way, step)]
-            ring_send(ring_s.at[way, slot, step], slot, way, step)
-
-    def weight_slot(slot):
+    def ring(slot, step):
+        phase(f"ring{slot}_{step}")
+        count = sum(step <= steps(slot, way) for way in range(2))
+        arrived(ring_r.at[0:count, slot, step - 1], ring_sem.at[slot, step - 1])
+        for way in range(2):
+            if step < steps(slot, way):
+                ring_s[way, slot, step] = ring_r[way, slot, step - 1] + part[slot, ring_target(slot, way, step)]
+                ring_send(ring_s.at[way, slot, step], slot, way, step)
+        if step == 4:
+            last = [steps(slot, way) - 1 for way in range(2)]
+            gw_out[slot] = part[slot, z] + ring_r[0, slot, last[0]] + ring_r[1, slot, last[1]]
+
+    def weight(slot):
+        phase(f"wait_ag{slot}")
         pair = peer_y(slot)
-        if slot > 0:
-            arrived(zg_r.at[slot], zg_sem.at[1, slot])
-        for o in range(1, NY):
-            arrived(gv_r.at[slot, peer_y(o)], ag_sem.at[1, slot, peer_y(o)])
+        arrived(gv_r.at[slot, 0 : NY - 1], ag_sem.at[1, slot])
         phase(f"weight{slot}")
         fresh = dot_fine_right(k_all, zg_r[slot])
         for block in range(NY):
             gv_r[slot, block] = gv_r[slot, block] + fade[block, pair] * fresh[128 * block : 128 * block + 128, :]
-        gv_own[pair] = gv_r[slot, y]
         gathered = gv_r[slot].reshape(512, 128).astype(BF16)
         part[slot] = dot(hid_all[...].reshape(512, 512), gathered).reshape(NZ, 64, 128)
         for way in range(2):
             ring_send(part.at[slot, ring_target(slot, way, 0)], slot, way, 0)
 
-    phase("wait_ag0")
-    weight_slot(0)
+    weight(0)
 
     phase("scan_z_f")
     wait_z(1, zr_f)
     scan_z(zr_f, zbs_f, False)
     zbr_f[z] = zbs_f[z]
     send_z(3, zbs_f, zbr_f)
-
-    phase("ring0_1")
-    for way in range(2):
-        ring_step(0, way, 1)
+    ring(0, 1)
+
+    phase("wait_zg_all")
+    arrived(zg_r.at[0 : NY - 1], zg_sem.at[1])
+    phase("grad_h")
+    for slot in range(PAIRS):
+        pair = peer_y(slot)
+        gv_own[pair] = gv_s[pair] + fade[y, pair] * dot_fine_right(k, zg_r[slot])
+    grad_v = jnp.concatenate([gv_own[pair].astype(BF16) for pair in range(PAIRS)], axis=1)
+    for part_now in range(4):
+        span = slice(512 * part_now, 512 * part_now + 512)
+        gh_s[:, :, :, span] = dot(grad_v, w[span, :], ((1,), (1,))).reshape(NX, 2, 16, 512)
+    send(gh_s.at[:, 1 - c], gh_r, d_sem.at[0, 0], d_sem.at[1, 0], c=1 - c)
+    drain_later(gh_r, d_sem.at[0, 0])
+
+    weight(1)
+    ring(0, 2)
+    weight(2)
+
+    phase("chip_pair")
+    arrived(gh_r, d_sem.at[1, 0])
+    gx_s[...] = gh_s[:, c] + gh_r[...]
+    for o in range(1, NX):
+        send(gx_s.at[peer_x(o)], gx_r.at[x], x_sem.at[0], x_sem.at[1], x=peer_x(o))
+    drain_later(gx_r.at[0 : NX - 1], x_sem.at[0])
+    gx_r[x] = gx_s[x]
+
+    weight(3)
 
     phase("back_y_f")
     wait_z(3, zbr_f)
@@ -389,105 +418,86 @@
     ybr_f[y] = ybs_f[y]
     send_y(4, ybs_f, ybr_f)
 
-    phase("ring0_2")
-    for way in range(2):
-        ring_step(0, way, 2)
-
-    for slot in range(1, PAIRS):
-        phase(f"wait_ag{slot}")
-        weight_slot(slot)
-
-    phase("grad_h")
-    grad_v = jnp.concatenate([gv_own[pair].astype(BF16) for pair in range(PAIRS)], axis=1)
-    for part_now in range(4):
-        span = slice(512 * part_now, 512 * part_now + 512)
-        gh_s[:, :, :, span] = dot(grad_v, w[span, :], ((1,), (1,))).reshape(NX, 2, 16, 512)
-    send(gh_s.at[:, 1 - c], gh_r, d_sem.at[0, 0], d_sem.at[1, 0], c=1 - c)
-
-    def ring_turn(step):
-        phase(f"ring{step}")
-        for slot in range(PAIRS):
-            for way in range(2):
-                ring_step(slot, way, step + 2 if slot == 0 else step)
-
-    ring_turn(1)
-    phase("chip_pair")
-    arrived(gh_r, d_sem.at[1, 0])
-    gx_s[...] = gh_s[:, c] + gh_r[...]
-    for o in range(1, NX):
-        send(gx_s.at[peer_x(o)], gx_r.at[x], x_sem.at[0, peer_x(o)], x_sem.at[1, x], x=peer_x(o))
-    gx_r[x] = gx_s[x]
-    ring_turn(2)
-
-    phase("grad_kq")
-    wait_y(4, ybr_f)
+    ring(1, 1)
+    ring(0, 3)
+    ring(2, 1)
+
+    phase("grad_k")
     gk = dot_fine_left(blend, q)
     gq = dot_fine_left(blend.T, k)
-    gap = jnp.zeros((8, 128), F32)
+    gap = row_sum[...]
     shared = jnp.zeros((8, 128), F32)
     head_row = lax.broadcasted_iota(jnp.int32, (8, 128), 0)
+    choosers = [jnp.where(head_row == 2 * pair + (lane8 >= 64).astype(jnp.int32), 1.0, 0.0) for pair in range(PAIRS)]
+
+    def gathered_rows(chooser, change):
+        return lax.dot_general(
+            chooser, change, (((1,), (1,)), ((), ())), precision=lax.Precision.HIGHEST, preferred_element_type=F32
+        )
+
+    for pair in range(PAIRS):
+        pull = ybr_b[pair] + row_of(gain_own, pair) * zg_r[lax.rem(pair + NY - y, NY)]
+        ybr_b[pair] = pull
+        val_f = vals[:, cols(pair)].astype(F32)
+        val_scaled = spread(to_end_t, pair) * val_f
+        gk = gk + dot_fine(val_scaled, pull, ((1,), (1,)))
+        whole = jnp.sum(val_scaled * dot_fine_right(k, pull), axis=0, keepdims=True)
+        shared = shared + jnp.sum(choosers[pair] * whole, axis=1, keepdims=True)
+        gv_own[pair] = val_f * gv_own[pair]
+    gk_out[...] = gk.astype(BF16)
+
+    ring(1, 2)
+    ring(3, 1)
+    ring(0, 4)
+    ring(2, 2)
+
+    phase("wait_carry")
+    wait_y(4, ybr_f)
+    phase("grad_q")
     for pair in range(PAIRS):
         carry = ybr_f[pair]
-        pull = ybr_b[pair] + row_of(gain_own, pair) * zg_r[lax.rem(pair + NY - y, NY)]
-        cot_f = cot[:, cols(pair)].astype(F32)
-        val_f = vals[:, cols(pair)].astype(F32)
-        cot_scaled = spread(from_start_t, pair) * cot_f
-        val_scaled = spread(to_end_t, pair) * val_f
+        cot_scaled = spread(from_start_t, pair) * cot[:, cols(pair)].astype(F32)
         gq = gq + dot_fine(cot_scaled, carry, ((1,), (1,)))
-        gk = gk + dot_fine(val_scaled, pull, ((1,), (1,)))
-        out_carried = dot_fine_right(q, carry)
-        from_state = dot_fine_right(k, pull)
-        owner = head_row == 2 * pair + (lane8 >= 64).astype(jnp.int32)
-        chooser = jnp.where(owner, 1.0, 0.0)
-        change = cot_scaled * out_carried - val_f * gv_own[pair]
-        gap = gap + lax.dot_general(
-            chooser, change, (((1,), (1,)), ((), ())),
-            precision=lax.Precision.HIGHEST, preferred_element_type=F32,
-        )
-        whole = jnp.sum(val_scaled * from_state, axis=0, keepdims=True)
-        whole = whole + row_of(factor, pair) * jnp.sum(carry * pull, axis=0, keepdims=True)
-        shared = shared + jnp.sum(chooser * whole, axis=1, keepdims=True)
-    gap = gap + row_sum[...]
+        change = cot_scaled * dot_fine_right(q, carry) - gv_own[pair]
+        gap = gap + gathered_rows(choosers[pair], change)
+        whole = row_of(factor, pair) * jnp.sum(carry * ybr_b[pair], axis=0, keepdims=True)
+        shared = shared + jnp.sum(choosers[pair] * whole, axis=1, keepdims=True)
     for shift in (1, 2, 4, 8, 16, 32, 64):
         gap = gap + jnp.where(lane8 < 128 - shift, pltpu.roll(gap, 128 - shift, 1), 0.0)
     gd_out[...] = (gap + shared) * (-rate / (1.0 + jnp.exp(-pre_v)))
-    gk_out[...] = gk.astype(BF16)
     gq_out[...] = gq.astype(BF16)
-    put(gk_out, gk_at, 0)
-    put(gq_out, gq_at, 1)
-    put(gd_out, gd_at, 2)
-
-    ring_turn(3)
+
+    ring(1, 3)
+    ring(3, 2)
+    ring(2, 3)
+    ring(1, 4)
+    ring(3, 3)
+
     phase("out_h")
-    for o in range(1, NX):
-        arrived(gx_r.at[peer_x(o)], x_sem.at[1, peer_x(o)])
+    arrived(gx_r.at[0 : NX - 1], x_sem.at[1])
     gh_out[...] = (gx_r[0] + gx_r[1] + gx_r[2] + gx_r[3]).astype(BF16)
-    put(gh_out, gh_at, 3)
-
-    ring_turn(4)
-    for slot in range(PAIRS):
-        last = [steps(slot, way) - 1 for way in range(2)]
-        gw_out[slot] = part[slot, z] + ring_r[0, slot, last[0]] + ring_r[1, slot, last[1]]
-        put(gw_out.at[slot], gw_at.at[:, pl.ds(pl.multiple_of(128 * peer_y(slot), 128), 128)], 4 + slot)
+
+    ring(2, 4)
+    ring(3, 4)
+    drain_later(part.at[0:PAIRS, 0 : NZ - 1], ring_sem.at[PAIRS, 0])
 
     phase("drain")
     for made in sent:
         made.wait_send()
-    for made in stored:
-        made.wait()
     stack.close()
 
 
 def store_all(*refs):
-    sems = refs[15]
-    taken = [pltpu.make_async_copy(refs[i], refs[10 + i], sems.at[0, i]) for i in range(5)]
-    given = [pltpu.make_async_copy(refs[10 + i], refs[5 + i], sems.at[1, i]) for i in range(5)]
-    for made in taken:
+    y = lax.axis_index("y")
+    sems = refs[10]
+    copies = [pltpu.make_async_copy(refs[i], refs[5 + i], sems.at[i]) for i in range(4)]
+    for slot in range(PAIRS):
+        pair = lax.rem(y + slot, PAIRS)
+        place = refs[9].at[:, pl.ds(pl.multiple_of(128 * pair, 128), 128)]
+        copies.append(pltpu.make_async_copy(refs[4].at[slot], place, sems.at[4 + slot]))
+    for made in copies:
         made.start()
-    for take, give in zip(taken, given):
-        take.wait()
-        give.start()
-    for made in given:
+    for made in copies:
         made.wait()
 
 
@@ -503,10 +513,10 @@
             jax.ShapeDtypeStruct((TOK, STATE), BF16),
             jax.ShapeDtypeStruct((HEADS, TOK), F32),
             jax.ShapeDtypeStruct((16, 2048), BF16),
-            jax.ShapeDtypeStruct((64, 512), F32),
+            jax.ShapeDtypeStruct((PAIRS, 64, 128), F32),
         ),
-        in_specs=[pl.BlockSpec(memory_space=pl.ANY)] * 7,
-        out_specs=[pl.BlockSpec(memory_space=pl.ANY)] * 5,
+        in_specs=[pl.BlockSpec(memory_space=pltpu.HBM)] * 7,
+        out_specs=[pl.BlockSpec(memory_space=pltpu.VMEM)] * 5,
         scratch_shapes=[
             *[f32(*y_box)] * 4,
             *[f32(*z_box)] * 4,
@@ -536,11 +546,6 @@
             f32(PAIRS, TOK, 128),
             pltpu.VMEM((TOK, 512), BF16),
             f32(HEADS, TOK),
-            pltpu.VMEM((TOK, STATE), BF16),
-            pltpu.VMEM((TOK, STATE), BF16),
-            f32(HEADS, TOK),
-            pltpu.VMEM((16, 2048), BF16),
-            f32(PAIRS, 64, 128),
             pltpu.VMEM((TOK, 2048), BF16),
             pltpu.VMEM((2048, 512), BF16),
             pltpu.VMEM((TOK, STATE), BF16),
@@ -549,37 +554,44 @@
             f32(1, HEADS),
             pltpu.VMEM((512, TOK), BF16),
             pltpu.VMEM((TOK, 512), BF16),
-            dma((2, 7, NY)),
-            dma((2, 4, NZ)),
-            dma((2, PAIRS, NY)),
-            dma((2, 2, PAIRS, 4)),
+            dma((2, 7)),
+            dma((2, 4)),
+            dma((2, PAIRS)),
+            dma((PAIRS + 1, 4)),
             dma((2, 2)),
-            dma((2, NX)),
+            dma((2,)),
             dma((7,)),
-            dma((2, NX)),
-            dma((8,)),
-            dma((2, NY)),
+            dma((2,)),
+            dma((2,)),
         ],
         compiler_params=pltpu.CompilerParams(
             collective_id=0, has_side_effects=True, vmem_limit_bytes=VMEM_LIMIT
         ),
         name="mixer_backward",
     )(
-        hidden,
-        value_weight,
-        key_vecs.reshape(TOK, STATE),
-        queries.reshape(TOK, STATE),
-        decay_pre.T,
-        decay_rate[None, :],
-        cotangent.reshape(TOK, 512).T,
+        *[
+            pltpu.with_memory_space_constraint(a, pltpu.HBM)
+            for a in (
+                hidden,
+                value_weight,
+                key_vecs.reshape(TOK, STATE),
+                queries.reshape(TOK, STATE),
+                decay_pre.T,
+                decay_rate[None, :],
+                cotangent.reshape(TOK, 512).T,
+            )
+        ]
     )
     gk, gq, gd, gh, gw = pl.pallas_call(
         store_all,
-        out_shape=tuple(jax.ShapeDtypeStruct(o.shape, o.dtype) for o in outs),
-        in_specs=[pl.BlockSpec(memory_space=pl.ANY)] * 5,
-        out_specs=[pl.BlockSpec(memory_space=pl.ANY)] * 5,
-        scratch_shapes=[*[pltpu.VMEM(o.shape, o.dtype) for o in outs], dma((2, 5))],
-        compiler_params=pltpu.CompilerParams(vmem_limit_bytes=VMEM_LIMIT),
+        out_shape=(
+            *[jax.ShapeDtypeStruct(o.shape, o.dtype) for o in outs[:4]],
+            jax.ShapeDtypeStruct((64, 512), F32),
+        ),
+        in_specs=[pl.BlockSpec(memory_space=pltpu.VMEM)] * 5,
+        out_specs=[pl.BlockSpec(memory_space=pltpu.HBM)] * 5,
+        scratch_shapes=[dma((8,))],
+        compiler_params=pltpu.CompilerParams(vmem_limit_bytes=2 * 1024 * 1024),
         name="store_all",
     )(*outs)
     return gk.reshape(TOK, 1, STATE), gq.reshape(TOK, 1, STATE), gd.T, gh, gw

time: 58.6 us -> 54.7 us (0.933)
  Pallas kernels: 57.6 us -> 54 us
    pallas_call x1, Pallas kernels: 55.9 us -> 53.2 us  [local(): pl.pallas_call(kernel, out_shape=(jax.ShapeDtypeStruct((TOK, STATE), BF16...]
    pallas_call x1, Pallas kernels: 1.72 us -> 0.77 us  [local(): pl.pallas_call(store_all, out_shape=(*[jax.ShapeDtypeStruct(o.shape, o.dt...]
where the time goes in v3:
time: 54.7 us; the launch traced here: 54.6 us
  Pallas kernels  54 us (99%)
  between operations  0.64 us (1%)
    pallas_call x1, Pallas kernels, local(): pl.pallas_call(kernel, out_shape=(jax.ShapeDtypeStruct((TOK, STATE), BF16...  53.2 us

profile of v3, /device:TPU:2, one launch (start us, length us, event | category | flops | bytes accessed | tf_op | source)
XLA Modules:
  0.0 54.6 jit_solution(3440024183200435858)
XLA Ops:
  0.6 53.2 %mixer_backward.1 = (bf16[128,128]{1,0:T(8,128)(2,1)S(1)}, bf16[128,128]{1,0:T(8,128)(2,1)S(1)}, f32[8,128]{1,0:T(8,128)S(1)}, bf16[16,2048]{1,0:T(8,128)(2,1)S(1)}, f32[4,64,128]{2,1,0:T(8,128)S(1)}) custom-call(bf16[128,2048]{1,0:T(8,128)(2,1)} %hid_at.1, bf16[2048,512]{1,0:T(8,128)(2,1)} %w_at.1, bf16[128,128]{1,0:T(8,128)(2,1)} %bitcast.11, ...), custom_call_target="tpu_custom_call" | custom-call | tf_op jit(solution)/shard_map/mixer_backward/pallas_call | solution.py:509
  53.8 0.8 %store_all.1 = (bf16[128,128]{1,0:T(8,128)(2,1)}, bf16[128,128]{1,0:T(8,128)(2,1)}, f32[8,128]{1,0:T(8,128)}, bf16[16,2048]{1,0:T(8,128)(2,1)}, f32[64,512]{1,0:T(8,128)}) custom-call(bf16[128,128]{1,0:T(8,128)(2,1)S(1)} %get-tuple-element.15.refs_0_, bf16[128,128]{1,0:T(8,128)(2,1)S(1)} %get-tuple-element.16.refs_1_, ...), custom_call_target="tpu_custom_call" | custom-call | tf_op jit(solution)/shard_map/store_all/pallas_call | solution.py:585

commit v4 on v3

--- a/solution.py
+++ b/solution.py
@@ -51,7 +51,7 @@
     gk_out, gq_out, gd_out, gh_out, gw_out,
     ys_b, yr_b, ys_f, yr_f, zs_b, zr_b, zs_f, zr_f,
     zbs_b, zbr_b, zbs_f, zbr_f, ybs_b, ybr_b, ybs_f, ybr_f,
-    hid_t, hid_p, hid_x, hid_c, hid_all, gv_s, gv_r, part, ring_s, ring_r,
+    hid_t, hid_p, hid_x, hid_c, hid_all, gv_s, gv_r, part, near_r, far_r, ring_s, ring_r,
     gh_s, gh_r, gx_s, gx_r, zg_s, zg_r, k_s, k_r, cum_s, cum_r, fade, gv_own, vals, row_sum,
     hid, w, k_in, q_in, pre, rate_in, cot_t, cot,
     y_sem, z_sem, ag_sem, ring_sem, d_sem, x_sem, in_sem, h_sem, zg_sem,
@@ -161,11 +161,12 @@
     loads[3].wait()
     q = q_in[...]
     q_t = q.astype(F32).T.astype(BF16)
-    upper = lax.broadcasted_iota(jnp.int32, (128, 128), 0) < 64
+    growth = jnp.concatenate(
+        [jnp.broadcast_to(from_start[head : head + 1, :], (64, 128)) for head in range(HEADS)], axis=0
+    )
+    pulls = dot_fine_right(q_t, growth * cot_t[...].astype(F32), ((1,), (1,)))
     for pair in range(PAIRS):
-        growth = jnp.where(upper, from_start[2 * pair : 2 * pair + 1, :], from_start[2 * pair + 1 : 2 * pair + 2, :])
-        scaled = growth * cot_t[cols(pair), :].astype(F32)
-        ys_b[pair, 0:128, :] = dot_fine_right(q_t, scaled, ((1,), (1,)))
+        ys_b[pair, 0:128, :] = pulls[:, cols(pair)]
         ys_b[pair, 128:136, :] = jnp.broadcast_to(row_of(factor, pair), (8, 128))
     yr_b[y] = ys_b[y]
     loads[4].wait()
@@ -196,9 +197,10 @@
     for half in range(2):
         span = slice(256 * half, 256 * half + 256)
         vals[:, span] = dot(hid[...], w[:, span]).astype(BF16)
+    scaled = jnp.concatenate([spread(to_end_t, pair) for pair in range(PAIRS)], axis=1) * vals[...].astype(F32)
+    states = dot_fine_right(k_t, scaled)
     for pair in range(PAIRS):
-        scaled = spread(to_end_t, pair) * vals[:, cols(pair)].astype(F32)
-        ys_f[pair, 0:128, :] = dot_fine_right(k_t, scaled)
+        ys_f[pair, 0:128, :] = states[:, cols(pair)]
         ys_f[pair, 128:136, :] = jnp.broadcast_to(row_of(factor, pair), (8, 128))
     yr_f[y] = ys_f[y]
 
@@ -338,30 +340,40 @@
             hid_all[across_x, c, :, cols(block)] = hid_x[across_x, block].astype(BF16)
             hid_all[across_x, 1 - c, :, cols(block)] = hid_c[across_x, block].astype(BF16)
 
-    def steps(slot, way):
-        return 4 if (slot + way) % 2 == 0 else 3
-
-    def ring_target(slot, way, step):
-        n = steps(slot, way)
-        return peer_z(n - step) if way == 0 else peer_z(NZ - n + step)
-
-    def ring_send(src, slot, way, step):
-        send(
-            src, ring_r.at[way, slot, step], ring_sem.at[PAIRS, 0], ring_sem.at[slot, step],
-            z=peer_z(1) if way == 0 else peer_z(NZ - 1),
+    spans = (slice(0, 32), slice(32, 64))
+
+    def ahead(way, o):
+        return peer_z(o) if way == 0 else peer_z(NZ - o)
+
+    def z_first(slot):
+        for way in range(2):
+            near, far = ahead(way, 1), ahead(way, 2)
+            send(part.at[slot, ahead(way, 3)], near_r.at[way, slot], ring_sem.at[2, 0], ring_sem.at[0, slot], z=near)
+            send(
+                part.at[slot, ahead(way, 4), spans[way]], far_r.at[way, slot], ring_sem.at[2, 0], ring_sem.at[0, slot],
+                z=far,
+            )
+        for way in range(2):
+            near = ahead(way, 1)
+            send(part.at[slot, near], ring_r.at[0, way, slot], ring_sem.at[2, 0], ring_sem.at[1, slot], z=near)
+
+    def z_second(slot):
+        phase(f"second{slot}")
+        arrived(part.at[slot, 0:3], ring_sem.at[0, slot])
+        for way in range(2):
+            far = ahead(way, 2)
+            mine = part[slot, far] + near_r[way, slot]
+            extra = mine[spans[way]] + far_r[way, slot]
+            ring_s[way, slot, spans[way]] = extra
+            ring_s[way, slot, spans[1 - way]] = mine[spans[1 - way]]
+            send(ring_s.at[way, slot], ring_r.at[1, way, slot], ring_sem.at[2, 0], ring_sem.at[1, slot], z=far)
+
+    def z_last(slot):
+        phase(f"last{slot}")
+        arrived(part.at[slot, 0:4], ring_sem.at[1, slot])
+        gw_out[slot] = (
+            part[slot, z] + ring_r[0, 0, slot] + ring_r[0, 1, slot] + ring_r[1, 0, slot] + ring_r[1, 1, slot]
         )
-
-    def ring(slot, step):
-        phase(f"ring{slot}_{step}")
-        count = sum(step <= steps(slot, way) for way in range(2))
-        arrived(ring_r.at[0:count, slot, step - 1], ring_sem.at[slot, step - 1])
-        for way in range(2):
-            if step < steps(slot, way):
-                ring_s[way, slot, step] = ring_r[way, slot, step - 1] + part[slot, ring_target(slot, way, step)]
-                ring_send(ring_s.at[way, slot, step], slot, way, step)
-        if step == 4:
-            last = [steps(slot, way) - 1 for way in range(2)]
-            gw_out[slot] = part[slot, z] + ring_r[0, slot, last[0]] + ring_r[1, slot, last[1]]
 
     def weight(slot):
         phase(f"wait_ag{slot}")
@@ -373,8 +385,7 @@
             gv_r[slot, block] = gv_r[slot, block] + fade[block, pair] * fresh[128 * block : 128 * block + 128, :]
         gathered = gv_r[slot].reshape(512, 128).astype(BF16)
         part[slot] = dot(hid_all[...].reshape(512, 512), gathered).reshape(NZ, 64, 128)
-        for way in range(2):
-            ring_send(part.at[slot, ring_target(slot, way, 0)], slot, way, 0)
+        z_first(slot)
 
     weight(0)
 
@@ -383,7 +394,7 @@
     scan_z(zr_f, zbs_f, False)
     zbr_f[z] = zbs_f[z]
     send_z(3, zbs_f, zbr_f)
-    ring(0, 1)
+    z_second(0)
 
     phase("wait_zg_all")
     arrived(zg_r.at[0 : NY - 1], zg_sem.at[1])
@@ -399,7 +410,13 @@
     drain_later(gh_r, d_sem.at[0, 0])
 
     weight(1)
-    ring(0, 2)
+
+    phase("back_y_f")
+    wait_z(3, zbr_f)
+    finish_plane(yr_f, ybs_f, zbr_f, False)
+    ybr_f[y] = ybs_f[y]
+    send_y(4, ybs_f, ybr_f)
+
     weight(2)
 
     phase("chip_pair")
@@ -412,74 +429,55 @@
 
     weight(3)
 
-    phase("back_y_f")
-    wait_z(3, zbr_f)
-    finish_plane(yr_f, ybs_f, zbr_f, False)
-    ybr_f[y] = ybs_f[y]
-    send_y(4, ybs_f, ybr_f)
-
-    ring(1, 1)
-    ring(0, 3)
-    ring(2, 1)
-
     phase("grad_k")
     gk = dot_fine_left(blend, q)
     gq = dot_fine_left(blend.T, k)
-    gap = row_sum[...]
-    shared = jnp.zeros((8, 128), F32)
-    head_row = lax.broadcasted_iota(jnp.int32, (8, 128), 0)
-    choosers = [jnp.where(head_row == 2 * pair + (lane8 >= 64).astype(jnp.int32), 1.0, 0.0) for pair in range(PAIRS)]
-
-    def gathered_rows(chooser, change):
-        return lax.dot_general(
-            chooser, change, (((1,), (1,)), ((), ())), precision=lax.Precision.HIGHEST, preferred_element_type=F32
-        )
-
-    for pair in range(PAIRS):
-        pull = ybr_b[pair] + row_of(gain_own, pair) * zg_r[lax.rem(pair + NY - y, NY)]
-        ybr_b[pair] = pull
-        val_f = vals[:, cols(pair)].astype(F32)
-        val_scaled = spread(to_end_t, pair) * val_f
-        gk = gk + dot_fine(val_scaled, pull, ((1,), (1,)))
-        whole = jnp.sum(val_scaled * dot_fine_right(k, pull), axis=0, keepdims=True)
-        shared = shared + jnp.sum(choosers[pair] * whole, axis=1, keepdims=True)
-        gv_own[pair] = val_f * gv_own[pair]
+    wide = lax.broadcasted_iota(jnp.int32, (8, 512), 1)
+    chooser = jnp.where(lax.broadcasted_iota(jnp.int32, (8, 512), 0) == wide // 64, 1.0, 0.0)
+    pull = jnp.concatenate(
+        [ybr_b[pair] + row_of(gain_own, pair) * zg_r[lax.rem(pair + NY - y, NY)] for pair in range(PAIRS)], axis=1
+    )
+    val_f = vals[...].astype(F32)
+    val_scaled = jnp.concatenate([spread(to_end_t, pair) for pair in range(PAIRS)], axis=1) * val_f
+    gk = gk + dot_fine(val_scaled, pull, ((1,), (1,)))
+    whole = jnp.sum(val_scaled * dot_fine_right(k, pull), axis=0, keepdims=True)
+    used = val_f * jnp.concatenate([gv_own[pair] for pair in range(PAIRS)], axis=1)
     gk_out[...] = gk.astype(BF16)
 
-    ring(1, 2)
-    ring(3, 1)
-    ring(0, 4)
-    ring(2, 2)
+    z_last(0)
+    z_second(1)
+    z_second(2)
+    z_second(3)
 
     phase("wait_carry")
     wait_y(4, ybr_f)
     phase("grad_q")
-    for pair in range(PAIRS):
-        carry = ybr_f[pair]
-        cot_scaled = spread(from_start_t, pair) * cot[:, cols(pair)].astype(F32)
-        gq = gq + dot_fine(cot_scaled, carry, ((1,), (1,)))
-        change = cot_scaled * dot_fine_right(q, carry) - gv_own[pair]
-        gap = gap + gathered_rows(choosers[pair], change)
-        whole = row_of(factor, pair) * jnp.sum(carry * ybr_b[pair], axis=0, keepdims=True)
-        shared = shared + jnp.sum(choosers[pair] * whole, axis=1, keepdims=True)
+    carry = jnp.concatenate([ybr_f[pair] for pair in range(PAIRS)], axis=1)
+    cot_scaled = jnp.concatenate([spread(from_start_t, pair) for pair in range(PAIRS)], axis=1) * cot[...].astype(F32)
+    gq = gq + dot_fine(cot_scaled, carry, ((1,), (1,)))
+    change = cot_scaled * dot_fine_right(q, carry) - used
+    high, low = halves(change)
+    lowest = (change - high.astype(F32) - low.astype(F32)).astype(BF16)
+    picked = chooser.astype(BF16)
+    gap = row_sum[...]
+    for level in (high, low, lowest):
+        gap = gap + dot(picked, level, ((1,), (1,)))
+    factors = jnp.concatenate([row_of(factor, pair) for pair in range(PAIRS)], axis=1)
+    whole = whole + factors * jnp.sum(carry * pull, axis=0, keepdims=True)
+    shared = jnp.sum(chooser * whole, axis=1, keepdims=True)
     for shift in (1, 2, 4, 8, 16, 32, 64):
         gap = gap + jnp.where(lane8 < 128 - shift, pltpu.roll(gap, 128 - shift, 1), 0.0)
     gd_out[...] = (gap + shared) * (-rate / (1.0 + jnp.exp(-pre_v)))
     gq_out[...] = gq.astype(BF16)
 
-    ring(1, 3)
-    ring(3, 2)
-    ring(2, 3)
-    ring(1, 4)
-    ring(3, 3)
-
     phase("out_h")
     arrived(gx_r.at[0 : NX - 1], x_sem.at[1])
     gh_out[...] = (gx_r[0] + gx_r[1] + gx_r[2] + gx_r[3]).astype(BF16)
 
-    ring(2, 4)
-    ring(3, 4)
-    drain_later(part.at[0:PAIRS, 0 : NZ - 1], ring_sem.at[PAIRS, 0])
+    z_last(1)
+    z_last(2)
+    z_last(3)
+    drain_later(part.at[0:PAIRS, 0 : NZ - 1], ring_sem.at[2, 0])
 
     phase("drain")
     for made in sent:
@@ -530,8 +528,10 @@
             f32(PAIRS, TOK, 128),
             f32(PAIRS, NY, TOK, 128),
             f32(PAIRS, NZ, 64, 128),
-            f32(2, PAIRS, 4, 64, 128),
-            f32(2, PAIRS, 4, 64, 128),
+            f32(2, PAIRS, 64, 128),
+            f32(2, PAIRS, 32, 128),
+            f32(2, PAIRS, 64, 128),
+            f32(2, 2, PAIRS, 64, 128),
             f32(NX, 2, 16, 2048),
             f32(NX, 16, 2048),
             f32(NX, 16, 2048),
@@ -557,7 +557,7 @@
             dma((2, 7)),
             dma((2, 4)),
             dma((2, PAIRS)),
-            dma((PAIRS + 1, 4)),
+            dma((3, PAIRS)),
             dma((2, 2)),
             dma((2,)),
             dma((7,)),

time: 54.7 us -> 51.5 us (0.941); the launches traced: 54.6 us -> 50.7 us
  Pallas kernels: 54 us -> 50 us
    pallas_call x1, Pallas kernels: 53.2 us -> 49.3 us  [local(): pl.pallas_call(kernel, out_shape=(jax.ShapeDtypeStruct((TOK, STATE), BF16...]
where the time goes in v4:
time: 51.5 us; the launch traced here: 50.7 us
  Pallas kernels  50 us (97%)
  between operations  0.64 us (1%)
    pallas_call x1, Pallas kernels, local(): pl.pallas_call(kernel, out_shape=(jax.ShapeDtypeStruct((TOK, STATE), BF16...  49.3 us

profile of v4, /device:TPU:2, one launch (start us, length us, event | category | flops | bytes accessed | tf_op | source)
XLA Modules:
  0.0 50.7 jit_solution(10083905671356707773)
XLA Ops:
  0.6 49.3 %mixer_backward.1 = (bf16[128,128]{1,0:T(8,128)(2,1)S(1)}, bf16[128,128]{1,0:T(8,128)(2,1)S(1)}, f32[8,128]{1,0:T(8,128)S(1)}, bf16[16,2048]{1,0:T(8,128)(2,1)S(1)}, f32[4,64,128]{2,1,0:T(8,128)S(1)}) custom-call(bf16[128,2048]{1,0:T(8,128)(2,1)} %hid_at.1, bf16[2048,512]{1,0:T(8,128)(2,1)} %w_at.1, bf16[128,128]{1,0:T(8,128)(2,1)} %bitcast.11, ...), custom_call_target="tpu_custom_call" | custom-call | tf_op jit(solution)/shard_map/mixer_backward/pallas_call | solution.py:507
  49.9 0.8 %store_all.1 = (bf16[128,128]{1,0:T(8,128)(2,1)}, bf16[128,128]{1,0:T(8,128)(2,1)}, f32[8,128]{1,0:T(8,128)}, bf16[16,2048]{1,0:T(8,128)(2,1)}, f32[64,512]{1,0:T(8,128)}) custom-call(bf16[128,128]{1,0:T(8,128)(2,1)S(1)} %get-tuple-element.15.refs_0_, bf16[128,128]{1,0:T(8,128)(2,1)S(1)} %get-tuple-element.16.refs_1_, ...), custom_call_target="tpu_custom_call" | custom-call | tf_op jit(solution)/shard_map/store_all/pallas_call | solution.py:585

commit v5 on v4

--- a/solution.py
+++ b/solution.py
@@ -49,12 +49,13 @@
 def kernel(
     hid_at, w_at, k_at, q_at, pre_at, rate_at, cot_at,
     gk_out, gq_out, gd_out, gh_out, gw_out,
-    ys_b, yr_b, ys_f, yr_f, zs_b, zr_b, zs_f, zr_f,
-    zbs_b, zbr_b, zbs_f, zbr_f, ybs_b, ybr_b, ybs_f, ybr_f,
-    hid_t, hid_p, hid_x, hid_c, hid_all, gv_s, gv_r, part, near_r, far_r, ring_s, ring_r,
-    gh_s, gh_r, gx_s, gx_r, zg_s, zg_r, k_s, k_r, cum_s, cum_r, fade, gv_own, vals, row_sum,
+    ys_f, yr_f, zs_b, zr_b, zs_f, zr_f,
+    zbs_b, zbr_b, zbs_f, zbr_f, ybs_f, ybr_f,
+    hid_t, hid_p, hid_x, hid_c, hid_all, gv_r, part, near_r, far_r, ring_s, ring_r,
+    gh_s, gh_r, gx_s, gx_r, zg_s, zg_r, k_s, k_r, q_s, q_r, q_t, cot_s, cot_r, cum_s, cum_r,
+    score, near_end, pulls, gains, suffix, reach, pull_own, gv_own, vals, row_sum,
     hid, w, k_in, q_in, pre, rate_in, cot_t, cot,
-    y_sem, z_sem, ag_sem, ring_sem, d_sem, x_sem, in_sem, h_sem, zg_sem,
+    y_sem, z_sem, rest_sem, ring_sem, d_sem, x_sem, in_sem, h_sem, zg_sem,
 ):
     z, y = lax.axis_index("z"), lax.axis_index("y")
     x, c = lax.axis_index("x"), lax.axis_index("c")
@@ -115,7 +116,7 @@
     loads = [
         pltpu.make_async_copy(src, dst, in_sem.at[i])
         for i, (src, dst) in enumerate(
-            [(pre_at, pre), (rate_at, rate_in), (cot_at, cot_t), (q_at, q_in), (k_at, k_in), (hid_at, hid), (w_at, w)]
+            [(cot_at, cot_t), (q_at, q_in), (pre_at, pre), (rate_at, rate_in), (k_at, k_in), (hid_at, hid), (w_at, w)]
         )
     ]
     for made in loads:
@@ -130,9 +131,25 @@
         pl.semaphore_signal(barrier, inc=1, device_id={"x": peer_x(o)}, device_id_type=MESH)
     pl.semaphore_signal(barrier, inc=1, device_id={"c": 1 - c}, device_id_type=MESH)
 
+    phase("widen")
+    loads[0].wait()
+    for pair in range(PAIRS):
+        cot_s[pair] = cot_t[cols(pair), :].astype(F32)
+    cot_r[y] = cot_s[...]
+    loads[1].wait()
+    q = q_in[...]
+    q_s[...] = q.astype(F32)
+    q_r[y] = q_s[...]
+    phase("barrier")
+    pl.semaphore_wait(barrier, NY + NZ + NX - 2)
+    share_y(3, q_s, q_r)
+    for o in range(1, NY):
+        send(cot_s.at[peer_y(o)], cot_r.at[y, peer_y(o)], y_sem.at[0, 0], y_sem.at[1, 0], y=peer_y(o))
+    drain_later(cot_r.at[0, 0 : NY - 1], y_sem.at[0, 0])
+
     phase("decay")
-    loads[0].wait()
-    loads[1].wait()
+    loads[2].wait()
+    loads[3].wait()
     pre_v = pre[...]
     square = lax.broadcasted_iota(jnp.int32, (8, 8), 0) == lax.broadcasted_iota(jnp.int32, (8, 8), 1)
     rate = jnp.sum(jnp.where(square, jnp.broadcast_to(rate_in[...], (8, 8)), 0.0), axis=1, keepdims=True)
@@ -156,27 +173,11 @@
     def row_of(gains, pair):
         return jnp.where(first_head, gains[2 * pair : 2 * pair + 1, :], gains[2 * pair + 1 : 2 * pair + 2, :])
 
-    phase("pull")
-    loads[2].wait()
-    loads[3].wait()
-    q = q_in[...]
-    q_t = q.astype(F32).T.astype(BF16)
-    growth = jnp.concatenate(
-        [jnp.broadcast_to(from_start[head : head + 1, :], (64, 128)) for head in range(HEADS)], axis=0
-    )
-    pulls = dot_fine_right(q_t, growth * cot_t[...].astype(F32), ((1,), (1,)))
-    for pair in range(PAIRS):
-        ys_b[pair, 0:128, :] = pulls[:, cols(pair)]
-        ys_b[pair, 128:136, :] = jnp.broadcast_to(row_of(factor, pair), (8, 128))
-    yr_b[y] = ys_b[y]
+    share_y(6, cum_s, cum_r)
     loads[4].wait()
     k = k_in[...]
     k_s[...] = k.astype(F32)
     k_r[y] = k_s[...]
-
-    phase("barrier")
-    pl.semaphore_wait(barrier, NY + NZ + NX - 2)
-    send_y(0, ys_b, yr_b)
 
     phase("hidden")
     loads[5].wait()
@@ -188,9 +189,6 @@
         send(hid_t.at[seat, peer_y(o)], hid_p.at[y], y_sem.at[0, 2], y_sem.at[1, 2], y=peer_y(o))
     drain_later(hid_p.at[0 : NY - 1], y_sem.at[0, 2])
     hid_p[y] = hid_t[seat, y]
-    share_y(5, k_s, k_r)
-    share_y(6, cum_s, cum_r)
-
     phase("values")
     loads[6].wait()
     k_t = k_s[...].T.astype(BF16)
@@ -203,28 +201,80 @@
         ys_f[pair, 0:128, :] = states[:, cols(pair)]
         ys_f[pair, 128:136, :] = jnp.broadcast_to(row_of(factor, pair), (8, 128))
     yr_f[y] = ys_f[y]
+    send_y(1, ys_f, yr_f)
+
+    share_y(5, k_s, k_r)
+
+    for o in range(1, PAIRS):
+        for way in range(2):
+            side = peer_y(1 + 2 * way)
+            pair = peer_y(1 + 2 * way + o)
+            send(cot_s.at[pair], cot_r.at[y, pair], rest_sem.at[2, 0], rest_sem.at[way, o - 1], y=side)
+    drain_later(cot_r.at[0:2, 0 : NY - 1], rest_sem.at[2, 0])
+    halves_of = (slice(0, 64), slice(64, 128))
+
+    def pass_on(way, o):
+        origin, side = peer_y(3 - 2 * way), peer_y(1 + 2 * way)
+        if o > 0:
+            arrived(cot_r.at[origin, peer_y(o)], rest_sem.at[way, o - 1])
+        if o != (1, 3)[way]:
+            half = cot_r.at[origin, peer_y(o), halves_of[way]]
+            send(half, half, y_sem.at[0, 7], y_sem.at[1, 7], y=side)
 
     phase("block")
     for pair in range(PAIRS):
         cot[:, cols(pair)] = cot_t[cols(pair), :].astype(F32).T.astype(BF16)
-    score = dot(k, q, ((1,), (1,)))
     causal = lax.broadcasted_iota(jnp.int32, (128, 128), 0) <= lane
     blend = jnp.zeros((128, 128), F32)
+    score_own = dot(k, q, ((1,), (1,)))
     for pair in range(PAIRS):
         cot_pair, val_pair = cot[:, cols(pair)], vals[:, cols(pair)]
-        inner = jnp.zeros((128, 128), F32)
         for side in range(2):
             head = 2 * pair + side
             mine = first_head if side == 0 else jnp.logical_not(first_head)
             across = jnp.where(causal, cum[head : head + 1, :] - cum_t[:, head : head + 1], 0.0)
             damping = jnp.where(causal, jnp.exp(across), 0.0)
-            weight = score * damping
             cot_head = jnp.where(mine, cot_pair.astype(F32), 0.0).astype(BF16)
-            inner = inner + dot_fine_left(weight, cot_head)
-            moved = dot(val_pair, cot_head, ((1,), (1,)))
-            blend = blend + moved * damping
-            row_sum[head : head + 1, :] = jnp.sum(moved * weight, axis=0, keepdims=True)
-        gv_s[pair] = inner
+            moved = dot(val_pair, cot_head, ((1,), (1,))) * damping
+            blend = blend + moved
+            row_sum[head : head + 1, :] = jnp.sum(moved * score_own, axis=0, keepdims=True)
+
+    upper = lax.broadcasted_iota(jnp.int32, (128, 128), 0) < 64
+
+    def rows_of(slot, block):
+        pair = peer_y(slot)
+        return [cum_r[block, pl.ds(2 * pair + side, 1), :] for side in range(2)]
+
+    def block_pull(slot, block):
+        first, second = rows_of(slot, block)
+        growth = jnp.where(upper, jnp.exp(first), jnp.exp(second))
+        pulls[slot, block] = dot_fine_right(q_t[block], growth * cot_r[block, peer_y(slot)], ((1,), (1,)))
+        gain = jnp.where(first_head, jnp.exp(first[:, 127:128]), jnp.exp(second[:, 127:128]))
+        gains[slot, block] = jnp.broadcast_to(gain, (8, 128))
+
+    def plane_chain(slot):
+        after = gain = None
+        for block in range(NY - 1, -1, -1):
+            suffix[slot, block] = jnp.zeros((128, 128), F32) if after is None else after
+            reach[slot, block] = jnp.ones((8, 128), F32) if gain is None else gain
+            here = gains[slot, block]
+            after = pulls[slot, block] if after is None else pulls[slot, block] + here[0:1, :] * after
+            gain = here if gain is None else gain * here
+        return after, gain
+
+    def block_values(slot, block):
+        rows = rows_of(slot, block)
+        tall = [jnp.broadcast_to(row, (128, 128)).T for row in rows]
+        near_end[slot, block] = jnp.exp(
+            jnp.where(first_head, rows[0][:, 127:128] - tall[0], rows[1][:, 127:128] - tall[1])
+        )
+        weights = []
+        for side in range(2):
+            across = jnp.where(causal, rows[side] - tall[side], 0.0)
+            weights.append(score[block] * jnp.where(causal, jnp.exp(across), 0.0))
+        cot_pair = cot_r[block, peer_y(slot)]
+        cots = jnp.concatenate([jnp.where(upper, cot_pair, 0.0), jnp.where(upper, 0.0, cot_pair)], axis=1)
+        gv_r[slot, block] = dot_fine_left(jnp.concatenate(weights, axis=1), cots.astype(BF16), ((1,), (1,)))
 
     def scan_plane(got, kept, z_send, reverse):
         state, gain = None, None
@@ -260,14 +310,25 @@
             here = got[block, 128:129, :]
             gain = here if gain is None else gain * here
 
-    phase("scan_y_b")
-    wait_y(0, yr_b)
-    scan_plane(yr_b, ybs_b, zs_b, True)
+    phase("first")
+    wait_y(6, cum_r)
+    wait_y(3, q_r)
+    arrived(cot_r.at[0, 0 : NY - 1], y_sem.at[1, 0])
+    phase("pulls0")
+    for block in range(NY):
+        q_t[block] = q_r[block].T.astype(BF16)
+    for block in range(NY):
+        block_pull(0, block)
+    state, gain = plane_chain(0)
+    for row in range(NZ):
+        zs_b[row, 0:ROWS, :] = state[row * ROWS : row * ROWS + ROWS, :]
+        zs_b[row, ROWS : ROWS + 8, :] = gain
     zr_b[z] = zs_b[z]
     send_z(0, zs_b, zr_b)
-    ybr_b[y] = ybs_b[y]
-    send_y(3, ybs_b, ybr_b)
-    send_y(1, ys_f, yr_f)
+    pass_on(0, 0)
+    pass_on(1, 0)
+    for slot in range(1, PAIRS):
+        block_pull(slot, y)
 
     phase("hidden_x")
     wait_y(2, hid_p)
@@ -276,46 +337,45 @@
     drain_later(hid_x.at[0 : NX - 1], h_sem.at[0])
     hid_x[x] = hid_p[...]
 
+    phase("scan_y_f")
+    wait_y(1, yr_f)
+    scan_plane(yr_f, ybs_f, zs_f, False)
+    zr_f[z] = zs_f[z]
+    send_z(1, zs_f, zr_f)
+
     phase("scan_z_b")
     wait_z(0, zr_b)
     scan_z(zr_b, zbs_b, True)
     zbr_b[z] = zbs_b[z]
     send_z(2, zbs_b, zbr_b)
 
-    phase("wait_suffix")
-    wait_y(3, ybr_b)
-    phase("gv_plane")
-    for pair in range(PAIRS):
-        gv_s[pair] = gv_s[pair] + spread(to_end_t, pair) * dot_fine_right(k, ybr_b[pair])
-
-    def share_slot(slot):
-        for o in range(1, NY):
-            send(gv_s.at[peer_y(o + slot)], gv_r.at[slot, y], ag_sem.at[0, slot], ag_sem.at[1, slot], y=peer_y(o))
-        drain_later(gv_r.at[slot, 0 : NY - 1], ag_sem.at[0, slot])
-        gv_r[slot, y] = gv_s[peer_y(slot)]
-
-    share_slot(0)
-    share_slot(1)
-
-    phase("fade")
-    wait_y(5, k_r)
-    wait_y(6, cum_r)
-    tail = jnp.zeros((8, 1), F32)
-    tail_own = jnp.zeros((8, 1), F32)
-    for block in range(NY - 1, -1, -1):
-        here = cum_r[block]
-        tail_own = jnp.where(y == block, tail, tail_own)
-        tail = tail + here[:, 127:128]
-        fade_t = jnp.exp(tail - here).T
-        for pair in range(PAIRS):
-            fade[block, pair] = spread(fade_t, pair)
-    gain_own = jnp.exp(jnp.broadcast_to(tail_own, (8, 128)))
-    k_all = k_r[...].reshape(512, 128).astype(BF16)
-
     phase("hidden_c")
     arrived(hid_x.at[0 : NX - 1], h_sem.at[1])
     send(hid_x, hid_c, d_sem.at[0, 1], d_sem.at[1, 1], c=1 - c)
     drain_later(hid_x, d_sem.at[0, 1])
+
+    phase("keys_far")
+    wait_y(5, k_r)
+    phase("values0")
+    for block in range(NY):
+        score[block] = dot(k_r[block].astype(BF16), q_r[block].astype(BF16), ((1,), (1,)))
+    for block in range(NY):
+        block_values(0, block)
+    for slot in range(1, PAIRS):
+        block_values(slot, y)
+
+    phase("pass1")
+    pass_on(0, 1)
+    pass_on(1, 1)
+    phase("scan_z_f")
+    wait_z(1, zr_f)
+    scan_z(zr_f, zbs_f, False)
+    zbr_f[z] = zbs_f[z]
+    send_z(3, zbs_f, zbr_f)
+
+    phase("pass2")
+    pass_on(0, 2)
+    pass_on(1, 2)
 
     phase("wait_zg")
     wait_z(2, zbr_b)
@@ -324,14 +384,6 @@
     for o in range(1, NY):
         send(zg_s, zg_r.at[NY - o], zg_sem.at[0], zg_sem.at[1], y=peer_y(o))
     drain_later(zg_r.at[0 : NY - 1], zg_sem.at[0])
-    share_slot(2)
-    share_slot(3)
-
-    phase("scan_y_f")
-    wait_y(1, yr_f)
-    scan_plane(yr_f, ybs_f, zs_f, False)
-    zr_f[z] = zs_f[z]
-    send_z(1, zs_f, zr_f)
 
     phase("hid_all")
     arrived(hid_c, d_sem.at[1, 1])
@@ -346,13 +398,14 @@
         return peer_z(o) if way == 0 else peer_z(NZ - o)
 
     def z_first(slot):
+        sems = (ring_sem.at[2, 0], ring_sem.at[0, slot])
         for way in range(2):
-            near, far = ahead(way, 1), ahead(way, 2)
-            send(part.at[slot, ahead(way, 3)], near_r.at[way, slot], ring_sem.at[2, 0], ring_sem.at[0, slot], z=near)
-            send(
-                part.at[slot, ahead(way, 4), spans[way]], far_r.at[way, slot], ring_sem.at[2, 0], ring_sem.at[0, slot],
-                z=far,
-            )
+            src = part.at[slot, ahead(way, 4), spans[way]]
+            send(src, far_r.at[way, slot], *sems, z=ahead(way, 2))
+        for way in range(2):
+            send(part.at[slot, ahead(way, 3)], near_r.at[way, slot], *sems, z=ahead(way, 1))
+
+    def z_direct(slot):
         for way in range(2):
             near = ahead(way, 1)
             send(part.at[slot, near], ring_r.at[0, way, slot], ring_sem.at[2, 0], ring_sem.at[1, slot], z=near)
@@ -375,33 +428,56 @@
             part[slot, z] + ring_r[0, 0, slot] + ring_r[0, 1, slot] + ring_r[1, 0, slot] + ring_r[1, 1, slot]
         )
 
+    def own_values(slot):
+        pair = peer_y(slot)
+        pull_now = suffix[slot, y] + reach[slot, y, 0:1, :] * zg_r[slot]
+        pull_own[pair] = pull_now
+        gv_own[pair] = gv_r[slot, y] + near_end[slot, y] * dot_fine_right(k, pull_now)
+
     def weight(slot):
-        phase(f"wait_ag{slot}")
-        pair = peer_y(slot)
-        arrived(gv_r.at[slot, 0 : NY - 1], ag_sem.at[1, slot])
         phase(f"weight{slot}")
-        fresh = dot_fine_right(k_all, zg_r[slot])
+        incoming = zg_r[slot]
         for block in range(NY):
-            gv_r[slot, block] = gv_r[slot, block] + fade[block, pair] * fresh[128 * block : 128 * block + 128, :]
+            pull_now = suffix[slot, block] + reach[slot, block, 0:1, :] * incoming
+            from_state = dot_fine_right(k_r[block].astype(BF16), pull_now)
+            gv_r[slot, block] = gv_r[slot, block] + near_end[slot, block] * from_state
         gathered = gv_r[slot].reshape(512, 128).astype(BF16)
         part[slot] = dot(hid_all[...].reshape(512, 512), gathered).reshape(NZ, 64, 128)
         z_first(slot)
 
+    own_values(0)
     weight(0)
-
-    phase("scan_z_f")
-    wait_z(1, zr_f)
-    scan_z(zr_f, zbs_f, False)
-    zbr_f[z] = zbs_f[z]
-    send_z(3, zbs_f, zbr_f)
-    z_second(0)
+    z_direct(0)
+
+    phase("pass3")
+    pass_on(0, 3)
+    pass_on(1, 3)
+    drain_later(cot_r.at[0, 0 : NY - 1], y_sem.at[0, 7])
+    phase("values_near")
+    for slot in range(1, PAIRS):
+        for o in (1, 3):
+            block_pull(slot, peer_y(o))
+            block_values(slot, peer_y(o))
+
+    phase("wait_opposite")
+    arrived(cot_r.at[0, 0 : NY - 1], y_sem.at[1, 7])
+    phase("values_far")
+    for slot in range(1, PAIRS):
+        block_pull(slot, peer_y(2))
+        block_values(slot, peer_y(2))
+        plane_chain(slot)
+    phase("back_y_f")
+    wait_z(3, zbr_f)
+    finish_plane(yr_f, ybs_f, zbr_f, False)
+    ybr_f[y] = ybs_f[y]
+    send_y(4, ybs_f, ybr_f)
 
     phase("wait_zg_all")
     arrived(zg_r.at[0 : NY - 1], zg_sem.at[1])
+    phase("own_values")
+    for slot in range(1, PAIRS):
+        own_values(slot)
     phase("grad_h")
-    for slot in range(PAIRS):
-        pair = peer_y(slot)
-        gv_own[pair] = gv_s[pair] + fade[y, pair] * dot_fine_right(k, zg_r[slot])
     grad_v = jnp.concatenate([gv_own[pair].astype(BF16) for pair in range(PAIRS)], axis=1)
     for part_now in range(4):
         span = slice(512 * part_now, 512 * part_now + 512)
@@ -410,14 +486,11 @@
     drain_later(gh_r, d_sem.at[0, 0])
 
     weight(1)
-
-    phase("back_y_f")
-    wait_z(3, zbr_f)
-    finish_plane(yr_f, ybs_f, zbr_f, False)
-    ybr_f[y] = ybs_f[y]
-    send_y(4, ybs_f, ybr_f)
-
+    z_second(0)
     weight(2)
+    weight(3)
+    for slot in range(1, PAIRS):
+        z_direct(slot)
 
     phase("chip_pair")
     arrived(gh_r, d_sem.at[1, 0])
@@ -427,16 +500,13 @@
     drain_later(gx_r.at[0 : NX - 1], x_sem.at[0])
     gx_r[x] = gx_s[x]
 
-    weight(3)
-
+    z_second(1)
     phase("grad_k")
     gk = dot_fine_left(blend, q)
     gq = dot_fine_left(blend.T, k)
     wide = lax.broadcasted_iota(jnp.int32, (8, 512), 1)
     chooser = jnp.where(lax.broadcasted_iota(jnp.int32, (8, 512), 0) == wide // 64, 1.0, 0.0)
-    pull = jnp.concatenate(
-        [ybr_b[pair] + row_of(gain_own, pair) * zg_r[lax.rem(pair + NY - y, NY)] for pair in range(PAIRS)], axis=1
-    )
+    pull = jnp.concatenate([pull_own[pair] for pair in range(PAIRS)], axis=1)
     val_f = vals[...].astype(F32)
     val_scaled = jnp.concatenate([spread(to_end_t, pair) for pair in range(PAIRS)], axis=1) * val_f
     gk = gk + dot_fine(val_scaled, pull, ((1,), (1,)))
@@ -444,10 +514,9 @@
     used = val_f * jnp.concatenate([gv_own[pair] for pair in range(PAIRS)], axis=1)
     gk_out[...] = gk.astype(BF16)
 
-    z_last(0)
-    z_second(1)
     z_second(2)
     z_second(3)
+    z_last(0)
 
     phase("wait_carry")
     wait_y(4, ybr_f)
@@ -516,16 +585,15 @@
         in_specs=[pl.BlockSpec(memory_space=pltpu.HBM)] * 7,
         out_specs=[pl.BlockSpec(memory_space=pltpu.VMEM)] * 5,
         scratch_shapes=[
-            *[f32(*y_box)] * 4,
+            *[f32(*y_box)] * 2,
             *[f32(*z_box)] * 4,
             *[f32(*z_back)] * 4,
-            *[f32(*y_back)] * 4,
+            *[f32(*y_back)] * 2,
             f32(NZ, NY, 64, TOK),
             f32(NY, 64, TOK),
             f32(NX, NY, 64, TOK),
             f32(NX, NY, 64, TOK),
             pltpu.VMEM((NX, 2, 64, 512), BF16),
-            f32(PAIRS, TOK, 128),
             f32(PAIRS, NY, TOK, 128),
             f32(PAIRS, NZ, 64, 128),
             f32(2, PAIRS, 64, 128),
@@ -540,9 +608,20 @@
             f32(NY, STATE, 128),
             f32(TOK, STATE),
             f32(NY, TOK, STATE),
+            f32(TOK, STATE),
+            f32(NY, TOK, STATE),
+            pltpu.VMEM((NY, STATE, TOK), BF16),
+            f32(PAIRS, 128, TOK),
+            f32(NY, PAIRS, 128, TOK),
             f32(HEADS, TOK),
             f32(NY, HEADS, TOK),
-            f32(NY, PAIRS, TOK, 128),
+            f32(NY, TOK, TOK),
+            f32(PAIRS, NY, TOK, 128),
+            f32(PAIRS, NY, STATE, 128),
+            f32(PAIRS, NY, 8, 128),
+            f32(PAIRS, NY, STATE, 128),
+            f32(PAIRS, NY, 8, 128),
+            f32(PAIRS, STATE, 128),
             f32(PAIRS, TOK, 128),
             pltpu.VMEM((TOK, 512), BF16),
             f32(HEADS, TOK),
@@ -554,9 +633,9 @@
             f32(1, HEADS),
             pltpu.VMEM((512, TOK), BF16),
             pltpu.VMEM((TOK, 512), BF16),
-            dma((2, 7)),
+            dma((2, 8)),
             dma((2, 4)),
-            dma((2, PAIRS)),
+            dma((3, 3)),
             dma((3, PAIRS)),
             dma((2, 2)),
             dma((2,)),

time: 51.5 us -> 50.1 us (0.973)
  Pallas kernels: 50 us -> 48.7 us
    pallas_call x1, Pallas kernels: 49.3 us -> 47.9 us  [local(): pl.pallas_call(kernel, out_shape=(jax.ShapeDtypeStruct((TOK, STATE), BF16...]
where the time goes in v5:
time: 50.1 us; the launch traced here: 49.3 us
  Pallas kernels  48.7 us (97%)
  between operations  0.64 us (1%)
    pallas_call x1, Pallas kernels, local(): pl.pallas_call(kernel, out_shape=(jax.ShapeDtypeStruct((TOK, STATE), BF16...  47.9 us

profile of v5, /device:TPU:2, one launch (start us, length us, event | category | flops | bytes accessed | tf_op | source)
XLA Modules:
  0.0 49.3 jit_solution(9345281128584460922)
XLA Ops:
  0.6 47.9 %mixer_backward.1 = (bf16[128,128]{1,0:T(8,128)(2,1)S(1)}, bf16[128,128]{1,0:T(8,128)(2,1)S(1)}, f32[8,128]{1,0:T(8,128)S(1)}, bf16[16,2048]{1,0:T(8,128)(2,1)S(1)}, f32[4,64,128]{2,1,0:T(8,128)S(1)}) custom-call(bf16[128,2048]{1,0:T(8,128)(2,1)} %hid_at.1, bf16[2048,512]{1,0:T(8,128)(2,1)} %w_at.1, bf16[128,128]{1,0:T(8,128)(2,1)} %bitcast.11, ...), custom_call_target="tpu_custom_call" | custom-call | tf_op jit(solution)/shard_map/mixer_backward/pallas_call | solution.py:576
  48.5 0.8 %store_all.1 = (bf16[128,128]{1,0:T(8,128)(2,1)}, bf16[128,128]{1,0:T(8,128)(2,1)}, f32[8,128]{1,0:T(8,128)}, bf16[16,2048]{1,0:T(8,128)(2,1)}, f32[64,512]{1,0:T(8,128)}) custom-call(bf16[128,128]{1,0:T(8,128)(2,1)S(1)} %get-tuple-element.15.refs_0_, bf16[128,128]{1,0:T(8,128)(2,1)S(1)} %get-tuple-element.16.refs_1_, ...), custom_call_target="tpu_custom_call" | custom-call | tf_op jit(solution)/shard_map/store_all/pallas_call | solution.py:664

commit v6 on v5

--- a/solution.py
+++ b/solution.py
@@ -55,7 +55,7 @@
     gh_s, gh_r, gx_s, gx_r, zg_s, zg_r, k_s, k_r, q_s, q_r, q_t, cot_s, cot_r, cum_s, cum_r,
     score, near_end, pulls, gains, suffix, reach, pull_own, gv_own, vals, row_sum,
     hid, w, k_in, q_in, pre, rate_in, cot_t, cot,
-    y_sem, z_sem, rest_sem, ring_sem, d_sem, x_sem, in_sem, h_sem, zg_sem,
+    y_sem, z_sem, rest_sem, ring_sem, d_sem, x_sem, in_sem, h_sem, zg_sem, near_sem,
 ):
     z, y = lax.axis_index("z"), lax.axis_index("y")
     x, c = lax.axis_index("x"), lax.axis_index("c")
@@ -125,7 +125,7 @@
     barrier = pltpu.get_barrier_semaphore()
     for o in range(1, NY):
         pl.semaphore_signal(barrier, inc=1, device_id={"y": peer_y(o)}, device_id_type=MESH)
-    for o in range(1, NZ):
+    for o in (1, NZ - 1):
         pl.semaphore_signal(barrier, inc=1, device_id={"z": peer_z(o)}, device_id_type=MESH)
     for o in range(1, NX):
         pl.semaphore_signal(barrier, inc=1, device_id={"x": peer_x(o)}, device_id_type=MESH)
@@ -141,7 +141,16 @@
     q_s[...] = q.astype(F32)
     q_r[y] = q_s[...]
     phase("barrier")
-    pl.semaphore_wait(barrier, NY + NZ + NX - 2)
+    pl.semaphore_wait(barrier, NY + NX + 1)
+
+    def tell_z(turn):
+        for o in (1, NZ - 1):
+            pl.semaphore_signal(near_sem.at[turn], inc=1, device_id={"z": peer_z(o)}, device_id_type=MESH)
+
+    def heard_z(turn):
+        pl.semaphore_wait(near_sem.at[turn], 2)
+
+    tell_z(0)
     share_y(3, q_s, q_r)
     for o in range(1, NY):
         send(cot_s.at[peer_y(o)], cot_r.at[y, peer_y(o)], y_sem.at[0, 0], y_sem.at[1, 0], y=peer_y(o))
@@ -179,6 +188,8 @@
     k_s[...] = k.astype(F32)
     k_r[y] = k_s[...]
 
+    heard_z(0)
+    tell_z(1)
     phase("hidden")
     loads[5].wait()
     for block in range(16):
@@ -221,6 +232,8 @@
             half = cot_r.at[origin, peer_y(o), halves_of[way]]
             send(half, half, y_sem.at[0, 7], y_sem.at[1, 7], y=side)
 
+    heard_z(1)
+    tell_z(2)
     phase("block")
     for pair in range(PAIRS):
         cot[:, cols(pair)] = cot_t[cols(pair), :].astype(F32).T.astype(BF16)
@@ -324,6 +337,7 @@
         zs_b[row, 0:ROWS, :] = state[row * ROWS : row * ROWS + ROWS, :]
         zs_b[row, ROWS : ROWS + 8, :] = gain
     zr_b[z] = zs_b[z]
+    heard_z(2)
     send_z(0, zs_b, zr_b)
     pass_on(0, 0)
     pass_on(1, 0)
@@ -477,6 +491,9 @@
     phase("own_values")
     for slot in range(1, PAIRS):
         own_values(slot)
+    weight(1)
+    z_second(0)
+    weight(2)
     phase("grad_h")
     grad_v = jnp.concatenate([gv_own[pair].astype(BF16) for pair in range(PAIRS)], axis=1)
     for part_now in range(4):
@@ -485,9 +502,6 @@
     send(gh_s.at[:, 1 - c], gh_r, d_sem.at[0, 0], d_sem.at[1, 0], c=1 - c)
     drain_later(gh_r, d_sem.at[0, 0])
 
-    weight(1)
-    z_second(0)
-    weight(2)
     weight(3)
     for slot in range(1, PAIRS):
         z_direct(slot)
@@ -495,7 +509,7 @@
     phase("chip_pair")
     arrived(gh_r, d_sem.at[1, 0])
     gx_s[...] = gh_s[:, c] + gh_r[...]
-    for o in range(1, NX):
+    for o in (2, 1, 3):
         send(gx_s.at[peer_x(o)], gx_r.at[x], x_sem.at[0], x_sem.at[1], x=peer_x(o))
     drain_later(gx_r.at[0 : NX - 1], x_sem.at[0])
     gx_r[x] = gx_s[x]
@@ -642,6 +656,7 @@
             dma((7,)),
             dma((2,)),
             dma((2,)),
+            pltpu.SemaphoreType.REGULAR((3,)),
         ],
         compiler_params=pltpu.CompilerParams(
             collective_id=0, has_side_effects=True, vmem_limit_bytes=VMEM_LIMIT

time: 50.1 us -> 48.4 us (0.966)
  Pallas kernels: 48.7 us -> 47.3 us
    pallas_call x1, Pallas kernels: 47.9 us -> 46.6 us  [local(): pl.pallas_call(kernel, out_shape=(jax.ShapeDtypeStruct((TOK, STATE), BF16...]
where the time goes in v6:
time: 48.4 us; the launch traced here: 48 us
  Pallas kernels  47.3 us (98%)
  between operations  0.64 us (1%)
    pallas_call x1, Pallas kernels, local(): pl.pallas_call(kernel, out_shape=(jax.ShapeDtypeStruct((TOK, STATE), BF16...  46.6 us

profile of v6, /device:TPU:2, one launch (start us, length us, event | category | flops | bytes accessed | tf_op | source)
XLA Modules:
  0.0 48.0 jit_solution(9855259431172076265)
XLA Ops:
  0.6 46.6 %mixer_backward.1 = (bf16[128,128]{1,0:T(8,128)(2,1)S(1)}, bf16[128,128]{1,0:T(8,128)(2,1)S(1)}, f32[8,128]{1,0:T(8,128)S(1)}, bf16[16,2048]{1,0:T(8,128)(2,1)S(1)}, f32[4,64,128]{2,1,0:T(8,128)S(1)}) custom-call(bf16[128,2048]{1,0:T(8,128)(2,1)} %hid_at.1, bf16[2048,512]{1,0:T(8,128)(2,1)} %w_at.1, bf16[128,128]{1,0:T(8,128)(2,1)} %bitcast.11, ...), custom_call_target="tpu_custom_call" | custom-call | tf_op jit(solution)/shard_map/mixer_backward/pallas_call | solution.py:590
  47.2 0.8 %store_all.1 = (bf16[128,128]{1,0:T(8,128)(2,1)}, bf16[128,128]{1,0:T(8,128)(2,1)}, f32[8,128]{1,0:T(8,128)}, bf16[16,2048]{1,0:T(8,128)(2,1)}, f32[64,512]{1,0:T(8,128)}) custom-call(bf16[128,128]{1,0:T(8,128)(2,1)S(1)} %get-tuple-element.15.refs_0_, bf16[128,128]{1,0:T(8,128)(2,1)S(1)} %get-tuple-element.16.refs_1_, ...), custom_call_target="tpu_custom_call" | custom-call | tf_op jit(solution)/shard_map/store_all/pallas_call | solution.py:679

commit v7 on v6

--- a/solution.py
+++ b/solution.py
@@ -209,8 +209,7 @@
     scaled = jnp.concatenate([spread(to_end_t, pair) for pair in range(PAIRS)], axis=1) * vals[...].astype(F32)
     states = dot_fine_right(k_t, scaled)
     for pair in range(PAIRS):
-        ys_f[pair, 0:128, :] = states[:, cols(pair)]
-        ys_f[pair, 128:136, :] = jnp.broadcast_to(row_of(factor, pair), (8, 128))
+        ys_f[pair] = states[:, cols(pair)]
     yr_f[y] = ys_f[y]
     send_y(1, ys_f, yr_f)
 
@@ -293,7 +292,7 @@
         state, gain = None, None
         order = range(NY - 1, -1, -1) if reverse else range(NY)
         for block in order:
-            value, here = got[block, 0:128, :], got[block, 128:129, :]
+            value, here = got[block], gains[0, block, 0:1, :]
             if state is None:
                 kept[block] = jnp.zeros((128, 128), F32)
                 state, gain = value, here
@@ -320,7 +319,7 @@
         gain = None
         for block in range(NY - 1, -1, -1) if reverse else range(NY):
             kept[block] = kept[block] + (incoming if gain is None else gain * incoming)
-            here = got[block, 128:129, :]
+            here = gains[0, block, 0:1, :]
             gain = here if gain is None else gain * here
 
     phase("first")
@@ -585,7 +584,7 @@
 def local(hidden, value_weight, key_vecs, queries, decay_pre, decay_rate, cotangent):
     dma = pltpu.SemaphoreType.DMA
     f32 = lambda *shape: pltpu.VMEM(shape, F32)
-    y_box, z_box = (NY, STATE + 8, 128), (NZ, ROWS + 8, 128)
+    y_box, z_box = (NY, STATE, 128), (NZ, ROWS + 8, 128)
     z_back, y_back = (NZ, ROWS, 128), (NY, STATE, 128)
     outs = pl.pallas_call(
         kernel,

time: 48.4 us -> 49.2 us (1.017)
  no operation moved by 1% of the time
where the time goes in v7:
time: 49.2 us; the launch traced here: 48.3 us
  Pallas kernels  47.7 us (97%)
  between operations  0.64 us (1%)
    pallas_call x1, Pallas kernels, local(): pl.pallas_call(kernel, out_shape=(jax.ShapeDtypeStruct((TOK, STATE), BF16...  46.9 us

profile of v7, /device:TPU:2, one launch (start us, length us, event | category | flops | bytes accessed | tf_op | source)
XLA Modules:
  0.0 48.3 jit_solution(14418599344317676018)
XLA Ops:
  0.6 46.9 %mixer_backward.1 = (bf16[128,128]{1,0:T(8,128)(2,1)S(1)}, bf16[128,128]{1,0:T(8,128)(2,1)S(1)}, f32[8,128]{1,0:T(8,128)S(1)}, bf16[16,2048]{1,0:T(8,128)(2,1)S(1)}, f32[4,64,128]{2,1,0:T(8,128)S(1)}) custom-call(bf16[128,2048]{1,0:T(8,128)(2,1)} %hid_at.1, bf16[2048,512]{1,0:T(8,128)(2,1)} %w_at.1, bf16[128,128]{1,0:T(8,128)(2,1)} %bitcast.11, ...), custom_call_target="tpu_custom_call" | custom-call | tf_op jit(solution)/shard_map/mixer_backward/pallas_call | solution.py:589
  47.6 0.8 %store_all.1 = (bf16[128,128]{1,0:T(8,128)(2,1)}, bf16[128,128]{1,0:T(8,128)(2,1)}, f32[8,128]{1,0:T(8,128)}, bf16[16,2048]{1,0:T(8,128)(2,1)}, f32[64,512]{1,0:T(8,128)}) custom-call(bf16[128,128]{1,0:T(8,128)(2,1)S(1)} %get-tuple-element.15.refs_0_, bf16[128,128]{1,0:T(8,128)(2,1)S(1)} %get-tuple-element.16.refs_1_, ...), custom_call_target="tpu_custom_call" | custom-call | tf_op jit(solution)/shard_map/store_all/pallas_call | solution.py:678

commit v8 on v6

--- a/solution.py
+++ b/solution.py
@@ -491,8 +491,8 @@
     phase("own_values")
     for slot in range(1, PAIRS):
         own_values(slot)
+    z_second(0)
     weight(1)
-    z_second(0)
     weight(2)
     phase("grad_h")
     grad_v = jnp.concatenate([gv_own[pair].astype(BF16) for pair in range(PAIRS)], axis=1)

time: 48.4 us -> 48.8 us (level)
  Pallas kernels: 47.3 us -> 48.1 us
    pallas_call x1, Pallas kernels: 46.6 us -> 47.3 us  [local(): pl.pallas_call(kernel, out_shape=(jax.ShapeDtypeStruct((TOK, STATE), BF16...]
where the time goes in v8:
time: 48.8 us; the launch traced here: 48.7 us
  Pallas kernels  48.1 us (99%)
  between operations  0.64 us (1%)
    pallas_call x1, Pallas kernels, local(): pl.pallas_call(kernel, out_shape=(jax.ShapeDtypeStruct((TOK, STATE), BF16...  47.3 us

profile of v8, /device:TPU:2, one launch (start us, length us, event | category | flops | bytes accessed | tf_op | source)
XLA Modules:
  0.0 48.7 jit_solution(14274380179001213960)
XLA Ops:
  0.6 47.3 %mixer_backward.1 = (bf16[128,128]{1,0:T(8,128)(2,1)S(1)}, bf16[128,128]{1,0:T(8,128)(2,1)S(1)}, f32[8,128]{1,0:T(8,128)S(1)}, bf16[16,2048]{1,0:T(8,128)(2,1)S(1)}, f32[4,64,128]{2,1,0:T(8,128)S(1)}) custom-call(bf16[128,2048]{1,0:T(8,128)(2,1)} %hid_at.1, bf16[2048,512]{1,0:T(8,128)(2,1)} %w_at.1, bf16[128,128]{1,0:T(8,128)(2,1)} %bitcast.11, ...), custom_call_target="tpu_custom_call" | custom-call | tf_op jit(solution)/shard_map/mixer_backward/pallas_call | solution.py:590
  48.0 0.8 %store_all.1 = (bf16[128,128]{1,0:T(8,128)(2,1)}, bf16[128,128]{1,0:T(8,128)(2,1)}, f32[8,128]{1,0:T(8,128)}, bf16[16,2048]{1,0:T(8,128)(2,1)}, f32[64,512]{1,0:T(8,128)}) custom-call(bf16[128,128]{1,0:T(8,128)(2,1)S(1)} %get-tuple-element.15.refs_0_, bf16[128,128]{1,0:T(8,128)(2,1)S(1)} %get-tuple-element.16.refs_1_, ...), custom_call_target="tpu_custom_call" | custom-call | tf_op jit(solution)/shard_map/store_all/pallas_call | solution.py:679
